TPU v7x, 128 devices: a whole 4x4x4 slice. The times are simulated.
128 devices in a mesh: st: 64 (over z, y, x), tp: 2 (over core).
Axes of the slice: x: 4, y: 4, z: 4, core: 2. Of those that a mesh axis runs over, the one named last changes fastest.
Arguments:
- tokens: bfloat16 [65536, 2048], P('st'), may hold values from -6 to 6
- store: bfloat16 [256, 64, 2048], P('st'), may hold values from -6 to 6
- passage_ids: int32 [1024, 4], P('st'), may hold values from 0 to 255, as said below
- w_query: bfloat16 [2048, 2048], P(None, 'tp'), may hold values from -0.125 to 0.125
- w_key: bfloat16 [2048, 512], P(None, 'tp'), may hold values from -0.125 to 0.125
- w_value: bfloat16 [2048, 512], P(None, 'tp'), may hold values from -0.125 to 0.125
- w_ret_query: bfloat16 [2048, 1024], P(None, 'tp'), may hold values from -0.125 to 0.125
- w_ret_key: bfloat16 [2048, 1024], P(None, 'tp'), may hold values from -0.125 to 0.125
- w_ret_value: bfloat16 [2048, 2048], P(None, 'tp'), may hold values from -0.125 to 0.125
- ret_rate: float32 [8], P('tp'), may hold values from 0.003 to 0.03
- ret_gain: float32 [2048], P('tp'), may hold values from 0.1 to 1.9
- gate_logit: float32 [2048], P('tp'), may hold values from -2 to 2
- out_grad: bfloat16 [65536, 2048], P('st', 'tp'), may hold values from -6 to 6
Outputs:
- grad_tokens: bfloat16 [65536, 2048], P(('st', 'tp'))
- grad_store: bfloat16 [256, 64, 2048], P(('st', 'tp'))
- grad_key_weight: float32 [2048, 512], P(None, 'tp')
Inputs may be any that keep to these rules, and one draw needn't show every extreme that they name: `passage_ids`: passage p lies on index p // 4 of st. The rows of one device name exactly 1 passage of every owner, so the 4 passages of a block differ.
All inputs are finite; a program needn't handle non-finite values.
Results may differ from a plain program's by a relative error of at most 0.012.
Values may be sent and summed in bfloat16 or wider, within the bound.
A program may use at most 192 MiB of HBM per device.

v0:
```python
import jax
import jax.numpy as jnp
from jax import lax
from jax.sharding import PartitionSpec as P

HEAD = 256
BLK = 64
KP = 4
MOST = 1


EPSILON = 1.0


def retention_grads(query_rows, key_rows, value_rows, rates, gains, cotangent):
    length = query_rows.shape[0]
    heads = rates.shape[0]
    queries = query_rows.reshape(length, heads, -1)
    keyset = key_rows.reshape(length, heads, -1)
    values = value_rows.reshape(length, heads, -1)
    positions = jnp.arange(length, dtype=jnp.float32)
    distance = positions[:, None] - positions[None, :]
    damping = jnp.where(
        distance >= 0.0, jnp.exp(-rates[:, None, None] * jnp.maximum(distance, 0.0)), 0.0
    ) * queries.shape[-1] ** (-0.5)
    raw = jnp.einsum("thd,shd->hts", queries, keyset, preferred_element_type=jnp.float32)
    weights = (raw * damping).astype(jnp.bfloat16)
    mixed = jnp.einsum("hts,she->the", weights, values, preferred_element_type=jnp.float32)
    inverse = lax.rsqrt(jnp.mean(mixed * mixed, axis=-1, keepdims=True) + EPSILON)
    scaled = cotangent.astype(jnp.float32).reshape(length, heads, -1) * gains.reshape(heads, -1)
    inner = jnp.mean(scaled * mixed, axis=-1, keepdims=True)
    grad_mixed = (inverse * scaled - inverse * inverse * inverse * mixed * inner).astype(
        jnp.bfloat16
    )
    grad_weights = (
        jnp.einsum("the,she->hts", grad_mixed, values, preferred_element_type=jnp.float32) * damping
    ).astype(jnp.bfloat16)
    grad_first = (
        jnp.einsum("hts,shd->thd", grad_weights, keyset, preferred_element_type=jnp.float32)
        .astype(jnp.bfloat16)
        .reshape(length, -1)
    )
    grad_second = (
        jnp.einsum("hts,thd->shd", grad_weights, queries, preferred_element_type=jnp.float32)
        .astype(jnp.bfloat16)
        .reshape(length, -1)
    )
    grad_third = (
        jnp.einsum("hts,the->she", weights, grad_mixed, preferred_element_type=jnp.float32)
        .astype(jnp.bfloat16)
        .reshape(length, -1)
    )
    return (grad_first, grad_second, grad_third)


def against_rows(left, weight):
    return lax.dot_general(
        left, weight, (((1,), (1,)), ((), ())), preferred_element_type=jnp.float32
    )


def across_rows(left, right):
    return lax.dot_general(
        left, right, (((0,), (0,)), ((), ())), preferred_element_type=jnp.float32
    )


def per_device(
    tokens,
    store,
    passage_ids,
    w_query,
    w_key,
    w_value,
    w_ret_query,
    w_ret_key,
    w_ret_value,
    ret_rate,
    ret_gain,
    gate_logit,
    out_grad,
):
    owners = lax.axis_size("st")
    pass_dev, plen, width = store.shape
    length = tokens.shape[0]
    kv_width = w_key.shape[1]
    kv_local = kv_width // HEAD
    group = w_query.shape[1] // HEAD // kv_local
    blocks = length // BLK
    slot_ids = passage_ids.reshape(-1)
    slot_count = slot_ids.shape[0]
    slot_owner = slot_ids // pass_dev
    slot_local = slot_ids % pass_dev
    order = jnp.arange(slot_count, dtype=jnp.int32)
    same_owner = slot_owner[:, None] == slot_owner[None, :]
    rank = jnp.sum(same_owner & (order[None, :] < order[:, None]), axis=1)
    position = slot_owner * MOST + rank
    cells = owners * MOST
    placed = jnp.arange(cells, dtype=jnp.int32)[:, None] == position[None, :]
    request = (jnp.sum(jnp.where(placed, slot_local[None, :] + 1, 0), axis=1) - 1).reshape(
        owners, MOST
    )
    incoming = lax.all_to_all(request, "st", split_axis=0, concat_axis=0, tiled=True)
    wanted = incoming.reshape(-1)
    valid = wanted >= 0
    safe = jnp.maximum(wanted, 0)
    placed_bf = placed.astype(jnp.bfloat16)
    store_rows = store.reshape(-1, width)
    nothing = jnp.zeros((), jnp.bfloat16)
    own_kv = jnp.concatenate(
        [
            jnp.dot(store_rows, w_key, preferred_element_type=jnp.float32).astype(jnp.bfloat16),
            jnp.dot(store_rows, w_value, preferred_element_type=jnp.float32).astype(jnp.bfloat16),
        ],
        axis=1,
    ).reshape(pass_dev, plen, 2 * kv_width)
    reply = jnp.where(valid[:, None, None], own_kv[safe], nothing).reshape(
        owners, MOST, plen, 2 * kv_width
    )
    arrived = lax.all_to_all(reply, "st", split_axis=0, concat_axis=0, tiled=True)
    slot_kv = (
        across_rows(placed_bf, arrived.reshape(cells, -1))
        .astype(jnp.bfloat16)
        .reshape(slot_count, plen, 2 * kv_width)
    )
    factor = HEAD ** (-0.5)
    gate = jax.nn.sigmoid(gate_logit)
    query_bf = jnp.dot(tokens, w_query, preferred_element_type=jnp.float32).astype(jnp.bfloat16)
    queries = query_bf.reshape(blocks, BLK, kv_local, group, HEAD)
    keys = slot_kv[:, :, :kv_width].reshape(blocks, KP * plen, kv_local, HEAD)
    values = slot_kv[:, :, kv_width:].reshape(blocks, KP * plen, kv_local, HEAD)
    scores = (
        jnp.einsum("btkgd,bskd->bkgts", queries, keys, preferred_element_type=jnp.float32) * factor
    )
    expo = jnp.exp(scores)
    probs = expo / jnp.sum(expo, axis=-1, keepdims=True)
    probs_bf = probs.astype(jnp.bfloat16)
    attn = jnp.einsum("bkgts,bskd->btkgd", probs_bf, values, preferred_element_type=jnp.float32)
    grad_attn = out_grad.astype(jnp.float32).reshape(
        blocks, BLK, kv_local, group, HEAD
    ) * gate.reshape(kv_local, group, HEAD)
    grad_attn_bf = grad_attn.astype(jnp.bfloat16)
    grad_probs = jnp.einsum(
        "btkgd,bskd->bkgts", grad_attn_bf, values, preferred_element_type=jnp.float32
    )
    delta = jnp.moveaxis(jnp.sum(grad_attn * attn, axis=-1), 1, 3)
    grad_scores = (probs * (grad_probs - delta[..., None]) * factor).astype(jnp.bfloat16)
    grad_query = (
        jnp.einsum("bkgts,bskd->btkgd", grad_scores, keys, preferred_element_type=jnp.float32)
        .astype(jnp.bfloat16)
        .reshape(length, -1)
    )
    grad_keys = (
        jnp.einsum("bkgts,btkgd->bskd", grad_scores, queries, preferred_element_type=jnp.float32)
        .astype(jnp.bfloat16)
        .reshape(slot_count, plen, kv_width)
    )
    grad_values = (
        jnp.einsum("bkgts,btkgd->bskd", probs_bf, grad_attn_bf, preferred_element_type=jnp.float32)
        .astype(jnp.bfloat16)
        .reshape(slot_count, plen, kv_width)
    )
    slot_grad = jnp.concatenate([grad_keys, grad_values], axis=2)
    outgoing = (
        jnp.dot(placed_bf, slot_grad.reshape(slot_count, -1), preferred_element_type=jnp.float32)
        .astype(jnp.bfloat16)
        .reshape(owners, MOST, plen, 2 * kv_width)
    )
    returned = lax.all_to_all(outgoing, "st", split_axis=0, concat_axis=0, tiled=True)
    matched = (jnp.arange(pass_dev, dtype=jnp.int32)[:, None] == wanted[None, :]).astype(
        jnp.bfloat16
    )
    passage_grad = jnp.dot(
        matched, returned.reshape(cells, -1), preferred_element_type=jnp.float32
    ).reshape(pass_dev * plen, 2 * kv_width)
    key_grad = passage_grad[:, :kv_width]
    upper = key_grad.astype(jnp.bfloat16)
    lower = (key_grad - upper.astype(jnp.float32)).astype(jnp.bfloat16)
    key_term = across_rows(store_rows, upper) + across_rows(store_rows, lower)
    grad_key_weight = lax.psum(key_term, "st")
    passage_bf = passage_grad.astype(jnp.bfloat16)
    grad_store = lax.psum_scatter(
        (
            against_rows(passage_bf[:, :kv_width], w_key)
            + against_rows(passage_bf[:, kv_width:], w_value)
        ).astype(jnp.bfloat16),
        "tp",
        scatter_dimension=0,
        tiled=True,
    ).astype(jnp.float32)
    grad_store = grad_store.astype(jnp.bfloat16).reshape(-1, plen, width)
    ret_query = jnp.dot(tokens, w_ret_query, preferred_element_type=jnp.float32).astype(
        jnp.bfloat16
    )
    ret_key = jnp.dot(tokens, w_ret_key, preferred_element_type=jnp.float32).astype(jnp.bfloat16)
    ret_value = jnp.dot(tokens, w_ret_value, preferred_element_type=jnp.float32).astype(
        jnp.bfloat16
    )
    grad_rq, grad_rk, grad_rv = retention_grads(
        ret_query, ret_key, ret_value, ret_rate, ret_gain, out_grad
    )
    total = against_rows(grad_query, w_query)
    total = total + against_rows(grad_rq, w_ret_query)
    total = total + against_rows(grad_rk, w_ret_key)
    grad_tokens = lax.psum_scatter(
        (total + against_rows(grad_rv, w_ret_value)).astype(jnp.bfloat16),
        "tp",
        scatter_dimension=0,
        tiled=True,
    )
    return (grad_tokens, grad_store, grad_key_weight)


def solution(mesh):
    return jax.shard_map(
        per_device,
        mesh=mesh,
        in_specs=(
            P("st", None),
            P("st", None, None),
            P("st", None),
            P(None, "tp"),
            P(None, "tp"),
            P(None, "tp"),
            P(None, "tp"),
            P(None, "tp"),
            P(None, "tp"),
            P("tp"),
            P("tp"),
            P("tp"),
            P("st", "tp"),
        ),
        out_specs=(P(("st", "tp"), None), P(("st", "tp"), None, None), P(None, "tp")),
        check_vma=False,
    )
```

profile of v0, /device:TPU:0, one launch (start us, length us, event | category | flops | bytes accessed | tf_op | source)
XLA Modules:
  0.0 347.4 jit_solution(12453826786444297427)
XLA Ops:
  10.1 11.5 %all-to-all-start = ((s32[64,1,1]{2,1,0:T(1,128)}), s32[64,1,1]{2,1,0:T(1,128)S(1)}, u32[]{:S(2)}, u32[]{:S(2)}) async-start(s32[64,1,1]{2,1,0:T(1,128)} %copy.72), calls=%async_computation | async-start | bytes 65536 | tf_op jit(solution)/shard_map/all_to_all | solution.py:103
  21.6 2.1 convolution_convert_fusion.9
  23.7 2.1 convolution_convert_fusion.10
  25.9 5.2 %all-to-all-done = s32[64,1,1]{2,1,0:T(1,128)S(1)} async-done(((s32[64,1,1]{2,1,0:T(1,128)}), s32[64,1,1]{2,1,0:T(1,128)S(1)}, u32[]{:S(2)}, u32[]{:S(2)}) %all-to-all-start) | async-done | bytes 288 | tf_op jit(solution)/shard_map/all_to_all | solution.py:103
  31.1 2.4 fusion.42
  33.5 2.8 gather_fusion
  37.5 4.5 %fusion.9 = bf16[64,1,64,512]{3,2,1,0:T(8,128)(2,1)} fusion(bf16[64,64,512]{2,1,0:T(8,128)(2,1)} %gather_fusion, pred[64]{0:T(512)(128)(4,1)S(1)} %compare_reduce_fusion), kind=kLoop, calls=%fused_computation.27 | loop fusion | flops 2097152 | bytes 8388672 | tf_op jit(solution)/shard_map/jit(_where)/select_n | solution.py:117
  42.0 5.8 %all-to-all-start.1 = ((bf16[64,1,64,512]{3,2,1,0:T(8,128)(2,1)}), bf16[64,1,64,512]{3,2,1,0:T(8,128)(2,1)}, u32[]{:S(2)}, u32[]{:S(2)}) async-start(bf16[64,1,64,512]{3,2,1,0:T(8,128)(2,1)} %fusion.9), calls=%async_computation.1 | async-start | bytes 8388608 | tf_op jit(solution)/shard_map/all_to_all | solution.py:120
  47.8 9.3 %convolution_convert_fusion.4 = bf16[1024,1024]{1,0:T(8,128)(2,1)} fusion(bf16[1024,2048]{1,0:T(8,128)(2,1)} %param.13, bf16[2048,1024]{1,0:T(8,128)(2,1)} %param.16), kind=kOutput, calls=%fused_computation.48 | convolution fusion | flops 4296015872 | bytes 10485760 | tf_op jit(solution)/shard_map/dot_general | solution.py:128
  57.1 4.1 %copy.81 = f32[1024,1024]{0,1:T(8,128)} copy(bf16[1024,1024]{1,0:T(8,128)(2,1)} %param.25) | data formatting | bytes 6291456 | tf_op jit(solution)/shard_map/convert_element_type | solution.py:139
  61.2 5.1 %reshape.312 = f32[16,64,4,256]{3,2,1,0:T(4,128)} reshape(bf16[1024,1024]{1,0:T(8,128)(2,1)} %param.25) | data formatting | bytes 6291456 | tf_op jit(solution)/shard_map/reshape | solution.py:139
  66.3 5.1 %reshape.313 = f32[16,64,1,4,256]{4,3,1,0,2:T(4,128)} reshape(bf16[1024,1024]{1,0:T(8,128)(2,1)} %param.25) | data formatting | bytes 6291456 | tf_op jit(solution)/shard_map/reshape | solution.py:139
  71.5 4.5 %reshape.310 = bf16[16,64,4,256]{3,2,1,0:T(4,128)(2,1)} reshape(bf16[1024,1024]{1,0:T(8,128)(2,1)} %convolution_convert_fusion.4) | data formatting | bytes 4194304 | tf_op jit(solution)/shard_map/reshape.1
  78.6 2.4 convolution_convert_fusion.7
  81.7 2.4 convolution_convert_fusion.8
  84.2 8.0 %multiply_convert_fusion.1 = bf16[4,1024,1024]{2,1,0:T(8,128)(2,1)} fusion(bf16[1024,4,128]{0,2,1:T(8,128)(2,1)S(1)} %bitcast.211, bf16[1024,4,128]{0,2,1:T(8,128)(2,1)S(1)} %bitcast.209, f32[1024,1024]{1,0:T(8,128)S(1)} %fusion.11, f32[4]{0:T(128)S(1)} %neg.8, pred[1024,1024]{1,0:T(8,128)(4,1)S(1)} %fusion.12), kind=kOutput, calls=%fused_computation.4 | convolution fusion | flops 1094713344 | bytes 15728656 | tf_op jit(solution)/shard_map/thd,shd->hts/dot_general | solution.py:26
  92.1 5.8 %convolution_convert_fusion.3 = bf16[1024,1024]{0,1:T(8,128)(2,1)} fusion(bf16[1024,2048]{1,0:T(8,128)(2,1)S(1)} %copy-done.20, bf16[2048,1024]{1,0:T(8,128)(2,1)S(1)} %copy-done.21), kind=kOutput, calls=%fused_computation.47 | convolution fusion | flops 4296015872 | bytes 10485760 | tf_op jit(solution)/shard_map/dot_general | solution.py:196
  97.9 2.8 all-to-all-done.1
  100.7 4.7 %copy.95 = bf16[8,8,64,512]{3,1,2,0:T(8,128)(2,1)S(1)} copy(bf16[8,8,64,512]{3,2,1,0:T(8,128)(2,1)} %bitcast.66) | data formatting | bytes 8388608
  105.4 1.3 convolution_convert_fusion.1
  106.7 1.6 copy.96
  108.7 1.8 copy-done.2
  112.7 2.1 bitcast_convert_fusion
  114.9 1.9 fusion
  116.8 3.1 fusion.3
  121.7 2.5 copy.98
  125.4 3.6 %copy.99 = bf16[8,8,64,512]{3,2,1,0:T(8,128)(2,1)} copy(bf16[8,8,64,512]{3,1,2,0:T(8,128)(2,1)S(1)} %bitcast.191) | data formatting | bytes 8388608
  129.0 8.5 %all-to-all-start.2 = ((bf16[64,1,64,512]{3,2,1,0:T(8,128)(2,1)}), bf16[64,1,64,512]{3,2,1,0:T(8,128)(2,1)}, u32[]{:S(2)}, u32[]{:S(2)}) async-start(bf16[64,1,64,512]{3,2,1,0:T(8,128)(2,1)} %bitcast.186), calls=%async_computation.3 | async-start | bytes 8388608 | tf_op jit(solution)/shard_map/all_to_all | solution.py:169
  137.6 8.2 %fusion.4 = (f32[1024,4]{0,1:T(4,128)S(1)}, f32[1024,4]{0,1:T(4,128)S(1)}, f32[4,256,1024]{2,1,0:T(8,128)S(1)}) fusion(f32[4,256]{1,0:T(4,128)S(1)} %mul.137, f32[1024,1024]{0,1:T(8,128)} %copy.81, bf16[1024,4,256]{0,2,1:T(8,128)(2,1)} %bitcast.207, bf16[4,1024,1024]{2,1,0:T(8,128)(2,1)} %multiply_convert_fusion.1), kind=kOutput, calls=%fused_computation.19 | convolution fusion | flops 2152718336 | bytes 18911232 | tf_op jit(solution)/shard_map/hts,she->the/dot_general | solution.py:28
  147.0 8.9 %multiply_convert_fusion = bf16[4,1024,1024]{2,1,0:T(8,128)(2,1)S(1)} fusion(bf16[1024,4,256]{0,2,1:T(8,128)(2,1)S(1)} %fusion.7, bf16[1024,4,256]{0,2,1:T(8,128)(2,1)} %bitcast.208, f32[1024,1024]{1,0:T(8,128)} %copy-done.12, f32[4]{0:T(128)S(1)} %copy-done.26, pred[1024,1024]{1,0:T(8,128)(4,1)} %copy-done.17), kind=kOutput, calls=%fused_computation.3 | convolution fusion | flops 2168455168 | bytes 17825808 | tf_op jit(solution)/shard_map/the,she->hts/dot_general | solution.py:36
  155.8 2.3 convolution_convert_fusion.5
  158.1 4.0 %convolution_convert_fusion.6 = bf16[4,128,1024]{2,1,0:T(8,128)(2,1)} fusion(bf16[1024,4,128]{0,2,1:T(8,128)(2,1)S(1)} %bitcast.210, bf16[4,1024,1024]{2,1,0:T(8,128)(2,1)S(1)} %multiply_convert_fusion), kind=kOutput, calls=%fused_computation.53 | convolution fusion | flops 1074266112 | bytes 10485760 | tf_op jit(solution)/shard_map/hts,shd->thd/dot_general | solution.py:39
  162.1 3.7 %convolution_convert_fusion.2 = bf16[4,256,1024]{2,1,0:T(8,128)(2,1)} fusion(bf16[1024,4,256]{0,2,1:T(8,128)(2,1)S(1)} %fusion.7, bf16[4,1024,1024]{2,1,0:T(8,128)(2,1)S(1)} %bitcast.201), kind=kOutput, calls=%fused_computation.46 | convolution fusion | flops 2148532224 | bytes 12582912 | tf_op jit(solution)/shard_map/hts,the->she/dot_general | solution.py:49
  165.8 26.9 %all-to-all-done.2 = bf16[64,1,64,512]{3,2,1,0:T(8,128)(2,1)} async-done(((bf16[64,1,64,512]{3,2,1,0:T(8,128)(2,1)}), bf16[64,1,64,512]{3,2,1,0:T(8,128)(2,1)}, u32[]{:S(2)}, u32[]{:S(2)}) %all-to-all-start.2) | async-done | bytes 4194336 | tf_op jit(solution)/shard_map/all_to_all | solution.py:169
  192.7 4.7 %copy.100 = bf16[8,8,64,512]{3,1,2,0:T(8,128)(2,1)S(1)} copy(bf16[8,8,64,512]{3,2,1,0:T(8,128)(2,1)} %bitcast.81) | data formatting | bytes 8388608
  197.4 1.5 fusion.37
  198.8 2.2 reshape.329
  201.0 1.4 fusion.33
  202.4 2.8 fusion.13
  205.3 7.0 %fusion.45 = f32[1024,2048]{1,0:T(8,128)} fusion(bf16[1024,512]{0,1:T(8,128)(2,1)} %bitcast.213, bf16[2048,512]{1,0:T(8,128)(2,1)S(1)} %copy-done), kind=kOutput, calls=%fused_computation.94 | convolution fusion | flops 2147483648 | bytes 11534336 | tf_op jit(solution)/shard_map/dot_general | solution.py:57
  212.3 7.0 %fusion.46 = f32[1024,2048]{1,0:T(8,128)} fusion(bf16[1024,1024]{0,1:T(8,128)(2,1)S(1)} %bitcast.215, bf16[2048,1024]{1,0:T(8,128)(2,1)S(1)} %copy-done.22), kind=kOutput, calls=%fused_computation.95 | convolution fusion | flops 4294967296 | bytes 14680064 | tf_op jit(solution)/shard_map/dot_general | solution.py:57
  220.1 1.8 copy.78
  221.9 1.8 copy.97
  224.3 1.5 fusion.14
  225.9 7.1 %fusion.44 = f32[1024,2048]{1,0:T(8,128)S(1)} fusion(bf16[1024,1024]{1,0:T(8,128)(2,1)} %bitcast.203, bf16[2048,1024]{1,0:T(8,128)(2,1)} %param.16), kind=kOutput, calls=%fused_computation.93 | convolution fusion | flops 4294967296 | bytes 14680064 | tf_op jit(solution)/shard_map/dot_general | solution.py:57
  233.0 12.1 %add_convert_fusion = bf16[1024,2048]{1,0:T(8,128)(2,1)} fusion(f32[1024,2048]{1,0:T(8,128)} %fusion.46, f32[1024,2048]{1,0:T(8,128)S(1)} %fusion.44, f32[1024,2048]{1,0:T(8,128)} %fusion.45, bf16[1024,512]{0,1:T(8,128)(2,1)} %bitcast.202, bf16[2048,512]{1,0:T(8,128)(2,1)} %param.20), kind=kOutput, calls=%fused_computation.6 | convolution fusion | flops 2155872256 | bytes 32505856 | tf_op jit(solution)/shard_map/dot_general | solution.py:57
  245.1 91.8 %all-reduce.2.cloned.1.call-done = f32[2048,256]{0,1:T(8,128)} async-done(((f32[2048,256]{0,1:T(8,128)}), f32[2048,256]{0,1:T(8,128)}) %all-reduce.2.cloned.1.call-update) | async-done | bytes 2097168 | tf_op jit(solution)/shard_map/psum | solution.py:180
  336.9 2.9 copy.86
  (94 shorter events, 14.9 us)
Async XLA Ops:
  8.0 69.6 %copy-start = (bf16[2048,512]{1,0:T(8,128)(2,1)S(1)}, bf16[2048,512]{1,0:T(8,128)(2,1)}, u32[]{:S(2)}) copy-start(bf16[2048,512]{1,0:T(8,128)(2,1)} %param.19) | copy-start | bytes 6291460
  10.1 21.0 %all-to-all-start = ((s32[64,1,1]{2,1,0:T(1,128)}), s32[64,1,1]{2,1,0:T(1,128)S(1)}, u32[]{:S(2)}, u32[]{:S(2)}) async-start(s32[64,1,1]{2,1,0:T(1,128)} %copy.72), calls=%async_computation | async-start | bytes 65536 | tf_op jit(solution)/shard_map/all_to_all | solution.py:103
  42.0 58.8 %all-to-all-start.1 = ((bf16[64,1,64,512]{3,2,1,0:T(8,128)(2,1)}), bf16[64,1,64,512]{3,2,1,0:T(8,128)(2,1)}, u32[]{:S(2)}, u32[]{:S(2)}) async-start(bf16[64,1,64,512]{3,2,1,0:T(8,128)(2,1)} %fusion.9), calls=%async_computation.1 | async-start | bytes 8388608 | tf_op jit(solution)/shard_map/all_to_all | solution.py:120
  66.3 5.1 %copy-start.23 = (f32[4]{0:T(128)S(1)}, f32[4]{0:T(128)}, u32[]{:S(2)}) copy-start(f32[4]{0:T(128)} %param.22) | copy-start | bytes 52
  66.3 5.1 %copy-start.18 = (f32[1024]{0:T(1024)S(1)}, f32[1024]{0:T(1024)}, u32[]{:S(2)}) copy-start(f32[1024]{0:T(1024)} %param.23) | copy-start | bytes 12292
  66.3 5.1 %copy-start.19 = (f32[1024]{0:T(1024)S(1)}, f32[1024]{0:T(1024)}, u32[]{:S(2)}) copy-start(f32[1024]{0:T(1024)} %param.24) | copy-start | bytes 12292
  71.5 12.7 %copy-start.25 = (f32[4]{0:T(128)}, f32[4]{0:T(128)S(1)}, u32[]{:S(2)}) copy-start(f32[4]{0:T(128)S(1)} %neg.8) | copy-start | bytes 52
  76.0 2.6 copy-start.20
  76.9 7.2 %copy-start.17 = (pred[1024,1024]{1,0:T(8,128)(4,1)}, pred[1024,1024]{1,0:T(8,128)(4,1)S(1)}, u32[]{:S(2)}) copy-start(pred[1024,1024]{1,0:T(8,128)(4,1)S(1)} %fusion.12) | copy-start | bytes 3145732
  78.6 5.6 %copy-start.12 = (f32[1024,1024]{1,0:T(8,128)}, f32[1024,1024]{1,0:T(8,128)S(1)}, u32[]{:S(2)}) copy-start(f32[1024,1024]{1,0:T(8,128)S(1)} %fusion.11) | copy-start | bytes 12582916
  78.6 3.1 copy-start.14
  81.7 2.5 copy-start.15
  84.2 8.0 %copy-start.21 = (bf16[2048,1024]{1,0:T(8,128)(2,1)S(1)}, bf16[2048,1024]{1,0:T(8,128)(2,1)}, u32[]{:S(2)}) copy-start(bf16[2048,1024]{1,0:T(8,128)(2,1)} %param.21) | copy-start | bytes 12582916
  108.3 2.2 copy-start.2
  108.7 2.9 copy-start.3
  110.5 2.2 copy-start.10
  112.7 2.2 copy-start.11
  119.9 1.4 copy-start.6
  129.0 63.6 %all-to-all-start.2 = ((bf16[64,1,64,512]{3,2,1,0:T(8,128)(2,1)}), bf16[64,1,64,512]{3,2,1,0:T(8,128)(2,1)}, u32[]{:S(2)}, u32[]{:S(2)}) async-start(bf16[64,1,64,512]{3,2,1,0:T(8,128)(2,1)} %bitcast.186), calls=%async_computation.3 | async-start | bytes 8388608 | tf_op jit(solution)/shard_map/all_to_all | solution.py:169
  137.5 199.4 %all-reduce.2.cloned.1.call-start = ((), (), s32[]{:S(2)}) async-start(), calls=%async_computation.7 | async-start | bytes 4194304 | tf_op jit(solution)/shard_map/psum | solution.py:180
  137.6 8.3 %copy-start.1 = (f32[1024,1024]{0,1:T(8,128)S(1)}, f32[1024,1024]{0,1:T(8,128)}, u32[]{:S(2)}) copy-start(f32[1024,1024]{0,1:T(8,128)} %copy.81) | copy-start | bytes 12582916
  145.8 1.1 copy-start.26
  145.8 16.2 %slice-start = ((s8[8388608]{0:T(1024)(128)(4,1)}), s8[4194304]{0:T(1024)(128)(4,1)S(1)}, s32[]{:S(2)}) async-start(s8[8388608]{0:T(1024)(128)(4,1)} %bitcast.200), calls=%async_computation.8 | async-start | bytes 8388608
  146.9 8.9 %copy-start.16 = (bf16[1024,512]{0,1:T(8,128)(2,1)S(1)}, bf16[1024,512]{0,1:T(8,128)(2,1)}, u32[]{:S(2)}) copy-start(bf16[1024,512]{0,1:T(8,128)(2,1)} %copy-done.15) | copy-start | bytes 3145732
  146.9 15.1 %slice-start.1 = ((s8[8388608]{0:T(1024)(128)(4,1)}), s8[4194304]{0:T(1024)(128)(4,1)S(1)}, s32[]{:S(2)}) async-start(s8[8388608]{0:T(1024)(128)(4,1)} %bitcast.200), calls=%async_computation.9 | async-start | bytes 8388608
  197.4 3.7 %copy-start.5 = (bf16[4,64,2048]{2,1,0:T(8,128)(2,1)S(1)}, bf16[4,64,2048]{2,1,0:T(8,128)(2,1)}, u32[]{:S(2)}) copy-start(bf16[4,64,2048]{2,1,0:T(8,128)(2,1)} %param.14) | copy-start | bytes 3145732
  205.2 134.5 %reduce-scatter.5.cloned.1.call-start = ((), (), s32[]{:S(2)}) async-start(), calls=%async_computation.6 | async-start | bytes 1572864 | tf_op jit(solution)/shard_map/reduce_scatter | solution.py:182
  205.3 7.0 %copy-start.22 = (bf16[2048,1024]{1,0:T(8,128)(2,1)S(1)}, bf16[2048,1024]{1,0:T(8,128)(2,1)}, u32[]{:S(2)}) copy-start(bf16[2048,1024]{1,0:T(8,128)(2,1)} %param.21) | copy-start | bytes 12582916
  205.3 7.0 %copy-start.24 = (bf16[4,256,1024]{2,1,0:T(8,128)(2,1)S(1)}, bf16[4,256,1024]{2,1,0:T(8,128)(2,1)}, u32[]{:S(2)}) copy-start(bf16[4,256,1024]{2,1,0:T(8,128)(2,1)} %convolution_convert_fusion.2) | copy-start | bytes 6291460
  212.3 7.1 %copy-start.4 = (bf16[64,64,256]{2,1,0:T(8,128)(2,1)S(1)}, bf16[64,64,256]{2,1,0:T(8,128)(2,1)}, u32[]{:S(2)}) copy-start(bf16[64,64,256]{2,1,0:T(8,128)(2,1)} %copy-done.3) | copy-start | bytes 6291460
  212.3 7.1 %copy-start.7 = (bf16[16,1,4,64,256]{4,3,2,0,1:T(8,128)(2,1)S(1)}, bf16[16,1,4,64,256]{4,3,2,0,1:T(8,128)(2,1)}, u32[]{:S(2)}) copy-start(bf16[16,1,4,64,256]{4,3,2,0,1:T(8,128)(2,1)} %copy-done.6) | copy-start | bytes 6291460
  220.1 3.6 %copy-start.8 = (f32[256,512]{1,0:T(8,128)S(1)}, f32[256,512]{1,0:T(8,128)}, u32[]{:S(2)}) copy-start(f32[256,512]{1,0:T(8,128)} %reshape.329) | copy-start | bytes 1572868
  220.1 3.7 %copy-start.9 = (bf16[2048,256]{1,0:T(8,128)(2,1)S(1)}, bf16[2048,256]{1,0:T(8,128)(2,1)}, u32[]{:S(2)}) copy-start(bf16[2048,256]{1,0:T(8,128)(2,1)} %param.17) | copy-start | bytes 3145732
  221.9 2.4 copy-start.13
  225.8 114.0 %reduce-scatter.3.cloned.1.call-start = ((), (), s32[]{:S(2)}) async-start(), calls=%async_computation.5 | async-start | bytes 6291456 | tf_op jit(solution)/shard_map/reduce_scatter | solution.py:205
Sparse Core Ops, SparseCore 0:
  205.4 131.4 all-reduce.1
Sparse Core Ops, SparseCore 1:
  225.9 9.5 reduce-scatter.4
  245.1 13.5 reduce-scatter.2
where the time goes:
time: 354 us; the launch traced here: 347 us
  waiting for transfers between devices  127 us (36%)
  matrix products  112 us (32%)
  local copies, waits for them, and re-layouts  54.9 us (16%)
  starting transfers between devices  26 us (7%)
  between operations  16.2 us (5%)
  other arithmetic  11.5 us (3%)
    psum x1, waiting for transfers between devices, per_device(): grad_key_weight = lax.psum(key_term, 'st')  91.8 us
    dot_general x6, matrix products, against_rows(): lax.dot_general(left, weight, (((1,), (1,)), ((), ())), preferred_element...  35.2 us
    unnamed x66, local copies, waits for them, and re-layouts  28 us
    all_to_all x1, waiting for transfers between devices, per_device(): lax.all_to_all(outgoing, 'st', split_axis=0, concat_axis=0, tiled=True)  26.9 us
    all_to_all x1, starting transfers between devices, per_device(): lax.all_to_all(request, 'st', split_axis=0, concat_axis=0, tiled=True)  11.5 us
    reshape x2, local copies, waits for them, and re-layouts, per_device(): out_grad.astype(jnp.float32).reshape(blocks, BLK, kv_local, group, HEAD)  10.2 us
    dot_general x1, matrix products, per_device(): jnp.dot(tokens, w_query, preferred_element_type=jnp.float32)  9.27 us
    dot_general x1, matrix products, retention_grads(): jnp.einsum('the,she->hts', grad_mixed, values, preferred_element_type=jnp...  8.86 us
  transfers between devices with their start and end apart: 6, of which 4 were waited for; matrix products, arithmetic and copies ran while one was open for 35% of the time, Pallas kernels for 0%

commit v1 on v0

v1 whole, which is shorter than its diff:
```python
import functools

import jax
import jax.numpy as jnp
from jax import lax
from jax.experimental import pallas as pl
from jax.experimental.pallas import tpu as pltpu
from jax.sharding import PartitionSpec as P

MESH = pl.DeviceIdType.MESH
HEAD = 256
BLK = 64
KP = 4
PLEN = 64
PASS_DEV = 4
OWNERS = 64
RET_KEY = 128
EPSILON = 1.0
VMEM_LIMIT = 60 * 1024 * 1024

STRIDES = (1, 4, 16)
CHANNELS = (
    (0, 0, 3, 0),
    (0, 3, 3, 1),
    (0, 6, 2, 2),
    (1, 0, 2, 0),
    (1, 2, 3, 1),
    (1, 5, 3, 2),
)
KEY_CHANNELS = (0, 1, 2)
VALUE_CHANNELS = (3, 4, 5)
STEPS = (1, 2, 3)
PARTS = ((0, 768), (768, 768), (1536, 512))


def nn(left, right):
    return jnp.dot(left, right, preferred_element_type=jnp.float32)


def nt(left, right):
    return lax.dot_general(
        left, right, (((1,), (1,)), ((), ())), preferred_element_type=jnp.float32
    )


def tn(left, right):
    return lax.dot_general(
        left, right, (((0,), (0,)), ((), ())), preferred_element_type=jnp.float32
    )


def coordinate(index, dim):
    return lax.rem(index // STRIDES[dim], 4)


def peer_of(me, dim, step):
    at = coordinate(me, dim)
    return me + (lax.rem(at + step, 4) - at) * STRIDES[dim]


def lines(turn):
    return turn, (turn + 1) % 3, (turn + 2) % 3


def line_barrier(me, sibling=None):
    barrier = pltpu.get_barrier_semaphore()
    for dim in range(3):
        for step in STEPS:
            pl.semaphore_signal(
                barrier, inc=1, device_id={"st": peer_of(me, dim, step)}, device_id_type=MESH
            )
    if sibling is None:
        pl.semaphore_wait(barrier, 9)
    else:
        pl.semaphore_signal(barrier, inc=1, device_id={"tp": sibling}, device_id_type=MESH)
        pl.semaphore_wait(barrier, 10)


def aligned(start, size, by=16):
    return pl.ds(pl.multiple_of(start, by), size)


def unit_place(unit):
    return (unit // 2) * 16, (unit % 2) * 128


def forward_kernel(
    need_ref,
    rate_ref,
    gain_ref,
    store_any,
    w_key_any,
    w_value_any,
    tokens_any,
    w_rq_any,
    w_rk_any,
    w_rv_any,
    w_q_any,
    grad_any,
    *rest,
):
    arrived = rest[:6]
    asked, q_any, grq_any, grk_any, grv_any = rest[6:11]
    table, outgoing, own = rest[11:17], rest[17:23], rest[23:29]
    (
        store,
        w_key,
        w_value,
        tokens,
        w_rq,
        w_rk,
        w_rv,
        w_q,
        grad,
        rq,
        rk,
        rv,
        q,
        grq,
        grk,
        grv,
        damp,
        weights,
        grad_weights,
        grad_y,
        load,
        leave,
        id_send,
        id_recv,
        send,
        recv,
    ) = rest[29:]
    me = lax.axis_index("st")
    loads = [
        pltpu.make_async_copy(source, target, load.at[at])
        for at, (source, target) in enumerate(
            (
                (store_any, store),
                (w_key_any, w_key),
                (w_value_any, w_value),
                (tokens_any, tokens),
                (w_rq_any, w_rq),
                (w_rk_any, w_rk),
                (w_rv_any, w_rv),
                (grad_any, grad),
                (w_q_any, w_q),
            )
        )
    ]
    for one in loads:
        one.start()
    line_barrier(me)
    names = []
    for dim in range(3):
        for step in STEPS:
            at = dim * 3 + step - 1
            one = pltpu.make_async_remote_copy(
                src_ref=need_ref.at[0],
                dst_ref=asked.at[at],
                send_sem=id_send.at[at],
                recv_sem=id_recv.at[at],
                device_id={"st": peer_of(me, dim, step)},
                device_id_type=MESH,
            )
            one.start()
            names.append(one)

    def remote(stage, channel, step, dim, source, target):
        return pltpu.make_async_remote_copy(
            src_ref=source,
            dst_ref=target,
            send_sem=send.at[stage, channel, step - 1],
            recv_sem=recv.at[stage, channel, step - 1],
            device_id={"st": peer_of(me, dim, step)},
            device_id_type=MESH,
        )

    def own_rows(kind, weight):
        made = nn(store[...], weight[...]).astype(jnp.bfloat16)
        for channel, (which, first, units, turn) in enumerate(CHANNELS):
            if which != kind:
                continue
            one, two, _ = lines(turn)
            at, beside = coordinate(me, one), coordinate(me, two)
            for passage in range(PASS_DEV):
                for unit in range(units):
                    row, column = unit_place(first + unit)
                    row = row + passage * PLEN
                    table[channel][beside, at, passage, unit] = made[
                        row : row + 16, column : column + 128
                    ]

    def first_stage(channels):
        copies = {}
        for channel in channels:
            one, two, _ = lines(CHANNELS[channel][3])
            at, beside = coordinate(me, one), coordinate(me, two)
            here = table[channel].at[beside, at]
            for step in STEPS:
                copies[channel, step] = remote(0, channel, step, one, here, here)
                copies[channel, step].start()
        return copies

    def second_stage(channels, before):
        copies = {}
        for channel in channels:
            _, two, _ = lines(CHANNELS[channel][3])
            for step in STEPS:
                before[channel, step].wait()
            here = table[channel].at[coordinate(me, two)]
            for step in STEPS:
                copies[channel, step] = remote(1, channel, step, two, here, here)
                copies[channel, step].start()
        return copies

    def third_stage(channels, before):
        copies = {}
        for channel in channels:
            one, two, last = lines(CHANNELS[channel][3])
            here = coordinate(me, last)
            for step in STEPS:
                before[channel, step].wait()

            @pl.loop(0, 16)
            def _(at):
                beside, along = at // 4, lax.rem(at, 4)
                owner = along * STRIDES[one] + beside * STRIDES[two] + here * STRIDES[last]
                own[channel][beside, along] = table[channel][beside, along, need_ref[0, 0, owner]]
                for step in STEPS:
                    row = last * 3 + (4 - step) - 1
                    outgoing[channel][step - 1, beside, along] = table[channel][
                        beside, along, asked[row, 0, owner]
                    ]

            for step in STEPS:
                copies[channel, step] = remote(
                    2,
                    channel,
                    step,
                    last,
                    outgoing[channel].at[step - 1],
                    arrived[channel].at[here],
                )
                copies[channel, step].start()
            copies[channel, 0] = pltpu.make_async_copy(
                own[channel], arrived[channel].at[here], leave.at[channel]
            )
            copies[channel, 0].start()
        return copies

    def project(weight, target):
        @pl.loop(0, weight.shape[1] // 256)
        def _(tile):
            columns = aligned(tile * 256, 256, 256)
            target[:, columns] = nn(tokens[...], weight[:, columns]).astype(jnp.bfloat16)

    def retention(start, stop):
        @pl.loop(start, stop)
        def _(head):
            rate = rate_ref[head]
            narrow = aligned(head * RET_KEY, RET_KEY, 128)
            wide = aligned(head * HEAD, HEAD, 256)
            rows = lax.broadcasted_iota(jnp.int32, (256, 256), 0)
            columns = lax.broadcasted_iota(jnp.int32, (256, 256), 1)
            for apart in range(4):
                distance = (rows - columns + 256 * apart).astype(jnp.float32)
                damp[apart] = jnp.where(
                    distance >= 0.0, jnp.exp(-rate * jnp.maximum(distance, 0.0)), 0.0
                ) * RET_KEY ** (-0.5)
            for i in range(4):
                block = pl.ds(i * 256, 256)
                upto = (i + 1) * 256
                for j in range(i + 1):
                    raw = nt(rq[block, narrow], rk[pl.ds(j * 256, 256), narrow])
                    weights[block, pl.ds(j * 256, 256)] = (raw * damp[i - j]).astype(jnp.bfloat16)
                y = nn(weights[block, pl.ds(0, upto)], rv[pl.ds(0, upto), wide])
                inverse = lax.rsqrt(jnp.mean(y * y, axis=1, keepdims=True) + EPSILON)
                scaled = grad[block, wide].astype(jnp.float32) * gain_ref[:, wide]
                inner = jnp.mean(scaled * y, axis=1, keepdims=True)
                grad_y[block, :] = (
                    inverse * scaled - (inverse * inverse * inverse * inner) * y
                ).astype(jnp.bfloat16)
                for j in range(i + 1):
                    raw = nt(grad_y[block, :], rv[pl.ds(j * 256, 256), wide])
                    grad_weights[block, pl.ds(j * 256, 256)] = (raw * damp[i - j]).astype(
                        jnp.bfloat16
                    )
                grq[block, narrow] = nn(
                    grad_weights[block, pl.ds(0, upto)], rk[pl.ds(0, upto), narrow]
                ).astype(jnp.bfloat16)
            for j in range(4):
                block = pl.ds(j * 256, 256)
                after = pl.ds(j * 256, 1024 - j * 256)
                grk[block, narrow] = tn(grad_weights[after, block], rq[after, narrow]).astype(
                    jnp.bfloat16
                )
                grv[block, wide] = tn(weights[after, block], grad_y[after, :]).astype(jnp.bfloat16)

    loads[0].wait()
    loads[1].wait()
    own_rows(0, w_key)
    keys = first_stage(KEY_CHANNELS)
    loads[2].wait()
    own_rows(1, w_value)
    values = first_stage(VALUE_CHANNELS)
    for one in names:
        one.wait()
    loads[3].wait()
    loads[4].wait()
    project(w_rq, rq)
    keys = second_stage(KEY_CHANNELS, keys)
    values = second_stage(VALUE_CHANNELS, values)
    loads[5].wait()
    project(w_rk, rk)
    loads[6].wait()
    project(w_rv, rv)
    loads[7].wait()
    retention(0, 1)
    keys = third_stage(KEY_CHANNELS, keys)
    retention(1, 2)
    values = third_stage(VALUE_CHANNELS, values)
    loads[8].wait()
    project(w_q, q)
    ends = [pltpu.make_async_copy(q, q_any, leave.at[6])]
    ends[0].start()
    retention(2, 4)
    for at, (source, target) in enumerate(((grq, grq_any), (grk, grk_any), (grv, grv_any))):
        one = pltpu.make_async_copy(source, target, leave.at[7 + at])
        one.start()
        ends.append(one)
    for one in list(keys.values()) + list(values.values()) + ends:
        one.wait()


def any_spec():
    return pl.BlockSpec(memory_space=pl.ANY)


def vmem_spec():
    return pl.BlockSpec(memory_space=pltpu.VMEM)


def smem_spec():
    return pl.BlockSpec(memory_space=pltpu.SMEM)


def forward(need, rate, gain, store, w_key, w_value, tokens, w_rq, w_rk, w_rv, w_q, grad):
    bf16, f32 = jnp.bfloat16, jnp.float32
    length, width = tokens.shape
    units = [channel[2] for channel in CHANNELS]
    out_shape = (
        [jax.ShapeDtypeStruct((4, 4, 4, n, 16, 128), bf16) for n in units]
        + [jax.ShapeDtypeStruct((9, 1, 128), jnp.int32)]
        + [
            jax.ShapeDtypeStruct((length, n), bf16)
            for n in (w_q.shape[1], w_rq.shape[1], w_rk.shape[1], w_rv.shape[1])
        ]
    )
    scratch = (
        [pltpu.VMEM((4, 4, 4, n, 16, 128), bf16) for n in units]
        + [pltpu.VMEM((3, 4, 4, n, 16, 128), bf16) for n in units]
        + [pltpu.VMEM((4, 4, n, 16, 128), bf16) for n in units]
        + [
            pltpu.VMEM(array.shape, array.dtype)
            for array in (store, w_key, w_value, tokens, w_rq, w_rk, w_rv, w_q, grad)
        ]
        + [
            pltpu.VMEM((length, n), bf16)
            for n in (w_rq.shape[1], w_rk.shape[1], w_rv.shape[1], w_q.shape[1])
        ]
        + [pltpu.VMEM((length, n), bf16) for n in (w_rq.shape[1], w_rk.shape[1], w_rv.shape[1])]
        + [
            pltpu.VMEM((4, 256, 256), f32),
            pltpu.VMEM((length, length), bf16),
            pltpu.VMEM((length, length), bf16),
            pltpu.VMEM((length, HEAD), bf16),
            pltpu.SemaphoreType.DMA((9,)),
            pltpu.SemaphoreType.DMA((10,)),
            pltpu.SemaphoreType.DMA((9,)),
            pltpu.SemaphoreType.DMA((9,)),
            pltpu.SemaphoreType.DMA((3, 6, 3)),
            pltpu.SemaphoreType.DMA((3, 6, 3)),
        ]
    )
    return pl.pallas_call(
        forward_kernel,
        name="fetch_and_retain",
        out_shape=out_shape,
        in_specs=[smem_spec(), smem_spec(), vmem_spec()] + [any_spec()] * 9,
        out_specs=[any_spec()] * 6 + [smem_spec()] + [any_spec()] * 4,
        scratch_shapes=scratch,
        compiler_params=pltpu.CompilerParams(
            collective_id=0, has_side_effects=True, vmem_limit_bytes=VMEM_LIMIT
        ),
    )(need, rate, gain, store, w_key, w_value, tokens, w_rq, w_rk, w_rv, w_q, grad)


PAIR = 2


def attention_kernel(ids_ref, gate_ref, q_ref, grad_ref, *rest):
    arrived, dq_ref, leaving = rest[:6], rest[6], rest[7:13]
    keys, values, queries, grads = rest[13:]
    factor = HEAD ** (-0.5)
    gate = jax.nn.sigmoid(gate_ref[...])
    for pair in range(PAIR):
        tokens = pl.ds(pair * BLK, BLK)
        where = []
        for slot in range(KP):
            owner = ids_ref[(pl.program_id(0) * PAIR + pair) * KP + slot] // PASS_DEV
            for channel, (kind, first, units, turn) in enumerate(CHANNELS):
                one, two, last = lines(turn)
                at = (coordinate(owner, last), coordinate(owner, two), coordinate(owner, one))
                where.append(at)
                target = values if kind else keys
                for unit in range(units):
                    row, column = unit_place(first + unit)
                    target[pair, pl.ds(slot * PLEN + row, 16), pl.ds(column, 128)] = arrived[
                        channel
                    ][at[0], at[1], at[2], unit]
        for head in range(4):
            columns = pl.ds(head * HEAD, HEAD)
            rows = pl.ds(head * BLK, BLK)
            queries[pair, rows, :] = q_ref[tokens, columns]
            grads[pair, rows, :] = (
                grad_ref[tokens, columns].astype(jnp.float32)
                * gate[:, head * HEAD : (head + 1) * HEAD]
            ).astype(jnp.bfloat16)
        expo = jnp.exp(nt(keys[pair], queries[pair]) * factor)
        probs = expo * (1.0 / jnp.sum(expo, axis=0, keepdims=True))
        probs_bf = probs.astype(jnp.bfloat16)
        grad_probs = nt(values[pair], grads[pair])
        delta = jnp.sum(probs_bf.astype(jnp.float32) * grad_probs, axis=0, keepdims=True)
        grad_scores = (probs * (grad_probs - delta) * factor).astype(jnp.bfloat16)
        key_grad = nn(grad_scores, queries[pair]).astype(jnp.bfloat16)
        value_grad = nn(probs_bf, grads[pair]).astype(jnp.bfloat16)
        query_grad = tn(grad_scores, keys[pair]).astype(jnp.bfloat16)
        for head in range(4):
            dq_ref[tokens, pl.ds(head * HEAD, HEAD)] = query_grad[head * BLK : (head + 1) * BLK]
        for slot in range(KP):
            for channel, (kind, first, units, turn) in enumerate(CHANNELS):
                at = where[slot * len(CHANNELS) + channel]
                made = value_grad if kind else key_grad
                for unit in range(units):
                    row, column = unit_place(first + unit)
                    row = row + slot * PLEN
                    leaving[channel][at[0], at[1], at[2], unit] = made[
                        row : row + 16, column : column + 128
                    ]


def attention(ids, gate, q, grad, arrived):
    bf16 = jnp.bfloat16
    length, width = q.shape
    units = [channel[2] for channel in CHANNELS]
    whole = [
        pl.BlockSpec((4, 4, 4, n, 16, 128), lambda step, ids: (0, 0, 0, 0, 0, 0)) for n in units
    ]
    rows = pl.BlockSpec((PAIR * BLK, width), lambda step, ids: (step, 0))
    return pl.pallas_call(
        attention_kernel,
        name="cross_attention",
        out_shape=[jax.ShapeDtypeStruct((length, width), bf16)]
        + [jax.ShapeDtypeStruct((4, 4, 4, n, 16, 128), bf16) for n in units],
        grid_spec=pltpu.PrefetchScalarGridSpec(
            num_scalar_prefetch=1,
            grid=(length // (PAIR * BLK),),
            in_specs=[pl.BlockSpec((1, width), lambda step, ids: (0, 0)), rows, rows] + whole,
            out_specs=[rows] + whole,
            scratch_shapes=[pltpu.VMEM((PAIR, 256, 256), bf16)] * 4,
        ),
        compiler_params=pltpu.CompilerParams(vmem_limit_bytes=VMEM_LIMIT),
    )(ids, gate, q, grad, *arrived)


def backward_kernel(
    need_ref,
    asked,
    store_any,
    w_key_any,
    w_value_any,
    dq_any,
    grq_any,
    grk_any,
    grv_any,
    w_q_any,
    w_rq_any,
    w_rk_any,
    w_rv_any,
    *rest,
):
    leaving = rest[:6]
    gt_ref, gs_ref, gw_ref = rest[6:9]
    own, third, sums, second, fewer, first_in = (
        rest[9:15],
        rest[15:21],
        rest[21:27],
        rest[27:33],
        rest[33:39],
        rest[39:45],
    )
    (
        store,
        w_key,
        w_value,
        dq,
        grq,
        grk,
        grv,
        w_q,
        w_rq,
        w_rk,
        w_rv,
        mine,
        theirs,
        passed,
        store_mine,
        store_theirs,
        store_passed,
        key_grad,
        value_grad,
        term,
        half,
        total,
        ar_first,
        ar_second,
        ar_third,
        out,
        load,
        near_send,
        near_recv,
        send,
        recv,
        ar_send,
        ar_recv,
    ) = rest[45:]
    me, core = lax.axis_index("st"), lax.axis_index("tp")
    sibling = 1 - core
    own_loads = []
    for channel, (_, _, _, turn) in enumerate(CHANNELS):
        here = coordinate(me, lines(turn)[2])
        own_loads.append(
            pltpu.make_async_copy(leaving[channel].at[here], own[channel], load.at[channel])
        )
    loads = [
        pltpu.make_async_copy(source, target, load.at[6 + at])
        for at, (source, target) in enumerate(
            (
                (dq_any, dq),
                (w_q_any, w_q),
                (grq_any, grq),
                (w_rq_any, w_rq),
                (grk_any, grk),
                (w_rk_any, w_rk),
                (grv_any, grv),
                (w_rv_any, w_rv),
                (store_any, store),
                (w_key_any, w_key),
                (w_value_any, w_value),
            )
        )
    ]
    line_barrier(me, sibling)

    def remote(stage, channel, step, dim, source, target):
        return pltpu.make_async_remote_copy(
            src_ref=source,
            dst_ref=target,
            send_sem=send.at[stage, channel, step - 1],
            recv_sem=recv.at[stage, channel, step - 1],
            device_id={"st": peer_of(me, dim, step)},
            device_id_type=MESH,
        )

    def third_stage(channels):
        copies = {}
        for channel in channels:
            last = lines(CHANNELS[channel][3])[2]
            at = coordinate(me, last)
            for step in STEPS:
                copies[channel, step] = remote(
                    0,
                    channel,
                    step,
                    last,
                    leaving[channel].at[lax.rem(at + step, 4)],
                    third[channel].at[step - 1],
                )
                copies[channel, step].start()
        return copies

    def second_stage(channels, before):
        copies = {}
        for channel in channels:
            one, two, last = lines(CHANNELS[channel][3])
            here = coordinate(me, last)
            own_loads[channel].wait()
            for step in STEPS:
                before[channel, step].wait()

            @pl.loop(0, 16)
            def _(at):
                beside, along = at // 4, lax.rem(at, 4)
                owner = along * STRIDES[one] + beside * STRIDES[two] + here * STRIDES[last]
                names = [need_ref[0, 0, owner]] + [
                    asked[last * 3 + step - 1, 0, owner] for step in STEPS
                ]
                rows = [own[channel][beside, along].astype(jnp.float32)] + [
                    third[channel][step - 1, beside, along].astype(jnp.float32) for step in STEPS
                ]
                for passage in range(PASS_DEV):
                    held = jnp.zeros_like(rows[0])
                    for name, row in zip(names, rows):
                        held = held + row * jnp.where(name == passage, 1.0, 0.0)
                    sums[channel][beside, along, passage] = held.astype(jnp.bfloat16)

            at = coordinate(me, two)
            for step in STEPS:
                copies[channel, step] = remote(
                    1,
                    channel,
                    step,
                    two,
                    sums[channel].at[lax.rem(at + step, 4)],
                    second[channel].at[step - 1],
                )
                copies[channel, step].start()
        return copies

    def first_stage(channels, before):
        copies = {}
        for channel in channels:
            one, two, _ = lines(CHANNELS[channel][3])
            for step in STEPS:
                before[channel, step].wait()
            here = coordinate(me, two)
            held = sums[channel][here].astype(jnp.float32)
            for step in STEPS:
                held = held + second[channel][step - 1].astype(jnp.float32)
            fewer[channel][...] = held.astype(jnp.bfloat16)
            at = coordinate(me, one)
            for step in STEPS:
                copies[channel, step] = remote(
                    2,
                    channel,
                    step,
                    one,
                    fewer[channel].at[lax.rem(at + step, 4)],
                    first_in[channel].at[step - 1],
                )
                copies[channel, step].start()
        return copies

    def passage_sums(channels, before, target):
        for channel in channels:
            _, first, units, turn = CHANNELS[channel]
            for step in STEPS:
                before[channel, step].wait()
            held = fewer[channel][coordinate(me, turn)].astype(jnp.float32)
            for step in STEPS:
                held = held + first_in[channel][step - 1].astype(jnp.float32)
            held = held.astype(jnp.bfloat16)
            for passage in range(PASS_DEV):
                for unit in range(units):
                    row, column = unit_place(first + unit)
                    target[pl.ds(passage * PLEN + row, 16), pl.ds(column, 128)] = held[
                        passage, unit
                    ]

    def near(at, source, target):
        return pltpu.make_async_remote_copy(
            src_ref=source,
            dst_ref=target,
            send_sem=near_send.at[at],
            recv_sem=near_recv.at[at],
            device_id={"tp": sibling},
            device_id_type=MESH,
        )

    length = dq.shape[0]
    part = length // 2

    def rows_of(left):
        return jnp.concatenate(
            [left[aligned(sibling * part, part), :], left[aligned(core * part, part), :]], axis=0
        )

    def token_grads(start, stop):
        @pl.loop(start, stop)
        def _(tile):
            columns = aligned(tile * 256, 256, 256)
            made = nt(rows_of(dq), w_q[columns, :])
            made = made + nt(rows_of(grq), w_rq[columns, :])
            made = made + nt(rows_of(grk), w_rk[columns, :])
            made = made + nt(rows_of(grv), w_rv[columns, :])
            theirs[tile] = made[:part].astype(jnp.bfloat16)
            mine[tile] = made[part:]
            near(tile, theirs.at[tile], passed.at[tile]).start()

    def token_ends(start, stop):
        @pl.loop(start, stop)
        def _(tile):
            near(tile, theirs.at[tile], passed.at[tile]).wait()
            columns = aligned(tile * 256, 256, 256)
            gt_ref[:, columns] = (mine[tile] + passed[tile].astype(jnp.float32)).astype(
                jnp.bfloat16
            )

    keys = third_stage(KEY_CHANNELS)
    values = third_stage(VALUE_CHANNELS)
    for one in loads + own_loads:
        one.start()
    for one in loads[:8]:
        one.wait()
    token_grads(0, 3)
    keys = second_stage(KEY_CHANNELS, keys)
    token_grads(3, 5)
    values = second_stage(VALUE_CHANNELS, values)
    token_grads(5, 6)
    keys = first_stage(KEY_CHANNELS, keys)
    token_grads(6, 8)
    values = first_stage(VALUE_CHANNELS, values)
    for one in loads[8:]:
        one.wait()
    passage_sums(KEY_CHANNELS, keys, key_grad)
    term[...] = tn(store[...], key_grad[...])
    half[...] = term[...].astype(jnp.bfloat16)

    def ar_copy(stage, place, step, dim, source, target):
        return pltpu.make_async_remote_copy(
            src_ref=source,
            dst_ref=target,
            send_sem=ar_send.at[stage, place, step - 1],
            recv_sem=ar_recv.at[stage, place, step - 1],
            device_id={"st": peer_of(me, dim, step)},
            device_id_type=MESH,
        )

    started = []
    for place, (start, size) in enumerate(PARTS):
        at = coordinate(me, place)
        quarter = size // 4
        for step in STEPS:
            there = lax.rem(at + step, 4)
            one = ar_copy(
                0,
                place,
                step,
                place,
                half.at[aligned(start + there * quarter, quarter)],
                ar_first.at[step - 1, pl.ds(start // 4, quarter)],
            )
            one.start()
            started.append(one)
    passage_sums(VALUE_CHANNELS, values, value_grad)
    store_rows = 2 * PLEN
    made = nt(
        jnp.concatenate(
            [
                key_grad[aligned(sibling * store_rows, store_rows), :],
                key_grad[aligned(core * store_rows, store_rows), :],
            ],
            axis=0,
        ),
        w_key[...],
    ) + nt(
        jnp.concatenate(
            [
                value_grad[aligned(sibling * store_rows, store_rows), :],
                value_grad[aligned(core * store_rows, store_rows), :],
            ],
            axis=0,
        ),
        w_value[...],
    )
    store_theirs[...] = made[:store_rows].astype(jnp.bfloat16)
    store_mine[...] = made[store_rows:]
    store_near = near(8, store_theirs, store_passed)
    store_near.start()
    stage = []
    for place, (start, size) in enumerate(PARTS):
        other = (place + 1) % 3
        at, beside = coordinate(me, place), coordinate(me, other)
        quarter, small = size // 4, size // 16
        base = start + at * quarter
        for step in STEPS:
            started[place * 3 + step - 1].wait()
        held = term[aligned(base, quarter), :]
        for step in STEPS:
            held = held + ar_first[step - 1, pl.ds(start // 4, quarter), :].astype(jnp.float32)
        total[pl.ds(start // 4, quarter), :] = held
        half[aligned(base, quarter), :] = held.astype(jnp.bfloat16)
        for step in STEPS:
            there = lax.rem(beside + step, 4)
            one = ar_copy(
                1,
                place,
                step,
                other,
                half.at[aligned(base + there * small, small)],
                ar_second.at[step - 1, pl.ds(start // 16, small)],
            )
            one.start()
            stage.append(one)
    token_ends(0, 4)
    started, stage = stage, []
    for place, (start, size) in enumerate(PARTS):
        _, other, last = lines(place)
        at, beside = coordinate(me, place), coordinate(me, other)
        quarter, small = size // 4, size // 16
        base = start + at * quarter + beside * small
        for step in STEPS:
            started[place * 3 + step - 1].wait()
        held = total[aligned(start // 4 + beside * small, small), :]
        for step in STEPS:
            held = held + ar_second[step - 1, pl.ds(start // 16, small), :].astype(jnp.float32)
        half[aligned(base, small), :] = held.astype(jnp.bfloat16)
        for step in STEPS:
            one = ar_copy(
                2,
                place,
                step,
                last,
                half.at[aligned(base, small)],
                ar_third.at[step - 1, pl.ds(start // 16, small)],
            )
            one.start()
            stage.append(one)
    token_ends(4, 8)
    started, stage = stage, []
    for place, (start, size) in enumerate(PARTS):
        other = (place + 1) % 3
        at, beside = coordinate(me, place), coordinate(me, other)
        quarter, small = size // 4, size // 16
        base = start + at * quarter + beside * small
        for step in STEPS:
            started[place * 3 + step - 1].wait()
        rows = pl.ds(start // 16, small)
        held = half[aligned(base, small), :].astype(jnp.float32) + ar_third[1, rows, :].astype(
            jnp.float32
        )
        held = held + (
            ar_third[0, rows, :].astype(jnp.float32) + ar_third[2, rows, :].astype(jnp.float32)
        )
        out[aligned(base, small), :] = held.astype(jnp.bfloat16)
        for step in STEPS:
            here = out.at[aligned(base, small)]
            one = ar_copy(3, place, step, other, here, here)
            one.start()
            stage.append(one)
    store_near.wait()
    gs_ref[...] = (store_mine[...] + store_passed[...].astype(jnp.float32)).astype(jnp.bfloat16)
    started, stage = stage, []
    for place, (start, size) in enumerate(PARTS):
        at = coordinate(me, place)
        quarter = size // 4
        base = start + at * quarter
        for step in STEPS:
            started[place * 3 + step - 1].wait()
        for step in STEPS:
            here = out.at[aligned(base, quarter)]
            one = ar_copy(4, place, step, place, here, here)
            one.start()
            stage.append(one)
    for one in stage:
        one.wait()
    gw_ref[...] = out[...].astype(jnp.float32)


def backward(
    need, asked, store, w_key, w_value, dq, grq, grk, grv, w_q, w_rq, w_rk, w_rv, leaving
):
    bf16, f32 = jnp.bfloat16, jnp.float32
    length, width = dq.shape[0], store.shape[1]
    units = [channel[2] for channel in CHANNELS]
    kv_width = w_key.shape[1]
    tiles = width // 256
    scratch = (
        [pltpu.VMEM((4, 4, n, 16, 128), bf16) for n in units]
        + [pltpu.VMEM((3, 4, 4, n, 16, 128), bf16) for n in units]
        + [pltpu.VMEM((4, 4, 4, n, 16, 128), bf16) for n in units]
        + [pltpu.VMEM((3, 4, 4, n, 16, 128), bf16) for n in units]
        + [pltpu.VMEM((4, 4, n, 16, 128), bf16) for n in units]
        + [pltpu.VMEM((3, 4, n, 16, 128), bf16) for n in units]
        + [
            pltpu.VMEM(array.shape, array.dtype)
            for array in (store, w_key, w_value, dq, grq, grk, grv, w_q, w_rq, w_rk, w_rv)
        ]
        + [
            pltpu.VMEM((tiles, length // 2, 256), f32),
            pltpu.VMEM((tiles, length // 2, 256), bf16),
            pltpu.VMEM((tiles, length // 2, 256), bf16),
            pltpu.VMEM((2 * PLEN, width), f32),
            pltpu.VMEM((2 * PLEN, width), bf16),
            pltpu.VMEM((2 * PLEN, width), bf16),
            pltpu.VMEM((PASS_DEV * PLEN, kv_width), bf16),
            pltpu.VMEM((PASS_DEV * PLEN, kv_width), bf16),
            pltpu.VMEM((width, kv_width), f32),
            pltpu.VMEM((width, kv_width), bf16),
            pltpu.VMEM((width // 4, kv_width), f32),
            pltpu.VMEM((3, width // 4, kv_width), bf16),
            pltpu.VMEM((3, width // 16, kv_width), bf16),
            pltpu.VMEM((3, width // 16, kv_width), bf16),
            pltpu.VMEM((width, kv_width), bf16),
            pltpu.SemaphoreType.DMA((17,)),
            pltpu.SemaphoreType.DMA((9,)),
            pltpu.SemaphoreType.DMA((9,)),
            pltpu.SemaphoreType.DMA((3, 6, 3)),
            pltpu.SemaphoreType.DMA((3, 6, 3)),
            pltpu.SemaphoreType.DMA((5, 3, 3)),
            pltpu.SemaphoreType.DMA((5, 3, 3)),
        ]
    )
    return pl.pallas_call(
        backward_kernel,
        name="return_and_reduce",
        out_shape=[
            jax.ShapeDtypeStruct((length // 2, width), bf16),
            jax.ShapeDtypeStruct((2 * PLEN, width), bf16),
            jax.ShapeDtypeStruct((width, kv_width), f32),
        ],
        in_specs=[smem_spec(), smem_spec()] + [any_spec()] * 17,
        out_specs=[vmem_spec()] * 3,
        scratch_shapes=scratch,
        compiler_params=pltpu.CompilerParams(
            collective_id=1, has_side_effects=True, vmem_limit_bytes=VMEM_LIMIT
        ),
    )(need, asked, store, w_key, w_value, dq, grq, grk, grv, w_q, w_rq, w_rk, w_rv, *leaving)


def per_device(
    tokens,
    store,
    passage_ids,
    w_query,
    w_key,
    w_value,
    w_ret_query,
    w_ret_key,
    w_ret_value,
    ret_rate,
    ret_gain,
    gate_logit,
    out_grad,
):
    width = store.shape[2]
    ids = passage_ids.reshape(-1)
    owners = jnp.arange(128, dtype=jnp.int32)
    need = jnp.sum(
        jnp.where(owners[:, None] == (ids // PASS_DEV)[None, :], (ids % PASS_DEV)[None, :], 0),
        axis=1,
    ).reshape(1, 1, 128)
    store_rows = store.reshape(-1, width)
    made = forward(
        need,
        ret_rate,
        ret_gain.reshape(1, -1),
        store_rows,
        w_key,
        w_value,
        tokens,
        w_ret_query,
        w_ret_key,
        w_ret_value,
        w_query,
        out_grad,
    )
    arrived, (asked, q, grq, grk, grv) = made[:6], made[6:]
    dq, *leaving = attention(ids, gate_logit.reshape(1, -1), q, out_grad, arrived)
    grad_tokens, grad_store, grad_key_weight = backward(
        need,
        asked,
        store_rows,
        w_key,
        w_value,
        dq,
        grq,
        grk,
        grv,
        w_query,
        w_ret_query,
        w_ret_key,
        w_ret_value,
        leaving,
    )
    return (grad_tokens, grad_store.reshape(-1, PLEN, width), grad_key_weight)


def solution(mesh):
    return jax.shard_map(
        per_device,
        mesh=mesh,
        in_specs=(
            P("st", None),
            P("st", None, None),
            P("st", None),
            P(None, "tp"),
            P(None, "tp"),
            P(None, "tp"),
            P(None, "tp"),
            P(None, "tp"),
            P(None, "tp"),
            P("tp"),
            P("tp"),
            P("tp"),
            P("st", "tp"),
        ),
        out_specs=(P(("st", "tp"), None), P(("st", "tp"), None, None), P(None, "tp")),
        check_vma=False,
    )
```

time: 354 us -> 141 us (0.40); the launches traced: 347 us -> 141 us
  Pallas kernels: 0 us -> 133 us
  waiting for transfers between devices: 127 us -> 0 us
  matrix products: 112 us -> 0 us
  local copies, waits for them, and re-layouts: 54.9 us -> 6.28 us
  starting transfers between devices: 26 us -> 0 us
  between operations: 16.2 us -> 0.69 us
  other arithmetic: 11.5 us -> 0.64 us
    pallas_call x0 -> x3, Pallas kernels: none -> 133 us  [the longest x1 67.7 us: backward(): pl.pallas_call(backward_kernel, name='return_and_reduce', out_shape=[jax....]
    dot_general x29 -> x0, matrix products: 112 us -> none  [the longest x6 35.2 us: against_rows(): lax.dot_general(left, weight, (((1,), (1,)), ((), ())), preferred_element...]
    psum x1 -> x0, waiting for transfers between devices: 91.8 us -> none  [per_device(): grad_key_weight = lax.psum(key_term, 'st')]
    all_to_all x3 -> x0, waiting for transfers between devices: 34.9 us -> none  [the longest x1 26.9 us: per_device(): lax.all_to_all(outgoing, 'st', split_axis=0, concat_axis=0, tiled=True)]
    all_to_all x3 -> x0, starting transfers between devices: 25.9 us -> none  [the longest x1 11.5 us: per_device(): lax.all_to_all(request, 'st', split_axis=0, concat_axis=0, tiled=True)]
    unnamed x66 -> x10, local copies, waits for them, and re-layouts: 28 us -> 6.19 us
    reshape x4 -> x1, local copies, waits for them, and re-layouts: 12.5 us -> 0.09 us  [per_device(): ids = passage_ids.reshape(-1)]
    convert_element_type x2 -> x0, local copies, waits for them, and re-layouts: 5.92 us -> none  [the longest x1 4.15 us: per_device(): out_grad.astype(jnp.float32).reshape(blocks, BLK, kv_local, group, HEAD)]
  transfers between devices with their start and end apart: 6 -> 0, of which waited for: 4 -> 0; matrix products, arithmetic and copies ran while one was open for 35% -> 0% of each run, Pallas kernels for 0% -> 0%
where the time goes in v1:
time: 141 us
  Pallas kernels  133 us (94%)
  local copies, waits for them, and re-layouts  6.28 us (4%)
    pallas_call x1, Pallas kernels, backward(): pl.pallas_call(backward_kernel, name='return_and_reduce', out_shape=[jax....  67.7 us
    pallas_call x1, Pallas kernels, forward(): pl.pallas_call(forward_kernel, name='fetch_and_retain', out_shape=out_sha...  51.7 us
    pallas_call x1, Pallas kernels, attention(): pl.pallas_call(attention_kernel, name='cross_attention', out_shape=[jax.S...  13.5 us
    unnamed x10, local copies, waits for them, and re-layouts  6.19 us

profile of v1, /device:TPU:0, one launch (start us, length us, event | category | flops | bytes accessed | tf_op | source)
XLA Modules:
  0.0 140.5 jit_solution(13632000242078350207)
XLA Ops:
  0.6 0.8 copy.18
  1.4 0.1 reshape.73.ids_ref
  1.5 0.0 copy-start.2
  1.5 0.6 select_reduce_fusion
  2.1 51.7 %fetch_and_retain.1 = (bf16[4,4,4,3,16,128]{5,4,3,2,1,0:T(8,128)(2,1)}, bf16[4,4,4,3,16,128]{5,4,3,2,1,0:T(8,128)(2,1)}, bf16[4,4,4,2,16,128]{5,4,3,2,1,0:T(8,12...) custom-call(s32[1,1,128]{2,1,0:T(1,128)} %bitcast.10, ...), custom_call_target="tpu_custom_call" | custom-call | tf_op jit(solution)/shard_map/fetch_and_retain/pallas_call | solution.py:385
  53.9 0.0 copy-done.2
  53.9 13.5 %cross_attention.1 = (bf16[1024,1024]{1,0:T(8,128)(2,1)}, bf16[4,4,4,3,16,128]{5,4,3,2,1,0:T(8,128)(2,1)}, bf16[4,4,4,3,16,128]{5,4,3,2,1,0:T(8,128)(2,1)}, bf16...) custom-call(s32[64]{0:T(128)} %copy-done.2, ...), custom_call_target="tpu_custom_call" | custom-call | tf_op jit(solution)/shard_map/cross_attention/pallas_call | solution.py:460
  67.4 67.7 %return_and_reduce.1 = (bf16[512,2048]{1,0:T(8,128)(2,1)}, bf16[128,2048]{1,0:T(8,128)(2,1)}, f32[2048,256]{1,0:T(8,128)}) custom-call(s32[1,1,128]{2,1,0:T(1,128)} %bitcast.11, s32[9,1,128]{2,1,0:T(1,128)} %get-tuple-element.24.asked, bf16[256,2048]{1,0:T(8,128)(2,1)} %bitcast.6, bf16[2048,256]{1,0:T(8,128)(2,1)} %w_key_any.3, ...), custom_call_target="tpu_custom_call" | custom-call | tf_op jit(solution)/shard_map/return_and_reduce/pallas_call | solution.py:914
  135.1 0.0 copy-start.1
  135.1 0.0 copy-start
  135.1 3.3 %copy.22 = bf16[512,2048]{1,0:T(8,128)(2,1)} copy(bf16[512,2048]{1,0:T(8,128)(2,1)} %get-tuple-element.50) | data formatting | bytes 4194304
  138.4 0.0 copy-done.1
  138.4 0.8 copy.23
  139.2 0.0 copy-done
  139.2 1.3 copy.24
  (1 shorter events, 0.0 us)
Async XLA Ops:
  1.5 52.4 %copy-start.2 = (s32[64]{0:T(128)}, s32[64]{0:T(128)S(1)}, u32[]{:S(2)}) copy-start(s32[64]{0:T(128)S(1)} %reshape.73.ids_ref) | copy-start | bytes 772
  135.1 3.3 %copy-start.1 = (bf16[128,2048]{1,0:T(8,128)(2,1)S(1)}, bf16[128,2048]{1,0:T(8,128)(2,1)}, u32[]{:S(2)}) copy-start(bf16[128,2048]{1,0:T(8,128)(2,1)} %get-tuple-element.43) | copy-start | bytes 1572868
  135.1 4.1 %copy-start = (f32[2048,256]{1,0:T(8,128)S(1)}, f32[2048,256]{1,0:T(8,128)}, u32[]{:S(2)}) copy-start(f32[2048,256]{1,0:T(8,128)} %get-tuple-element.52) | copy-start | bytes 6291460

commit v2 on v1

--- a/solution.py
+++ b/solution.py
@@ -18,7 +18,6 @@
 EPSILON = 1.0
 VMEM_LIMIT = 60 * 1024 * 1024
 
-STRIDES = (1, 4, 16)
 CHANNELS = (
     (0, 0, 3, 0),
     (0, 3, 3, 1),
@@ -49,17 +48,22 @@
     )
 
 
+def stride(dim):
+    return (9 * dim * dim - 3 * dim + 2) // 2
+
+
 def coordinate(index, dim):
-    return lax.rem(index // STRIDES[dim], 4)
+    return lax.rem(index // stride(dim), 4)
 
 
 def peer_of(me, dim, step):
     at = coordinate(me, dim)
-    return me + (lax.rem(at + step, 4) - at) * STRIDES[dim]
+    return me + (lax.rem(at + step, 4) - at) * stride(dim)
 
 
 def lines(turn):
-    return turn, (turn + 1) % 3, (turn + 2) % 3
+    first = turn + lax.axis_index("tp")
+    return lax.rem(first, 3), lax.rem(first + 1, 3), lax.rem(first + 2, 3)
 
 
 def line_barrier(me, sibling=None):
@@ -221,10 +225,10 @@
             for step in STEPS:
                 before[channel, step].wait()
 
-            @pl.loop(0, 16)
+            @pl.loop(0, 16, unroll=4)
             def _(at):
                 beside, along = at // 4, lax.rem(at, 4)
-                owner = along * STRIDES[one] + beside * STRIDES[two] + here * STRIDES[last]
+                owner = along * stride(one) + beside * stride(two) + here * stride(last)
                 own[channel][beside, along] = table[channel][beside, along, need_ref[0, 0, owner]]
                 for step in STEPS:
                     row = last * 3 + (4 - step) - 1
@@ -395,7 +399,7 @@
     )(need, rate, gain, store, w_key, w_value, tokens, w_rq, w_rk, w_rv, w_q, grad)
 
 
-PAIR = 2
+PAIR = 4
 
 
 def attention_kernel(ids_ref, gate_ref, q_ref, grad_ref, *rest):
@@ -403,21 +407,22 @@
     keys, values, queries, grads = rest[13:]
     factor = HEAD ** (-0.5)
     gate = jax.nn.sigmoid(gate_ref[...])
+    core = lax.axis_index("tp")
+    where = {}
     for pair in range(PAIR):
         tokens = pl.ds(pair * BLK, BLK)
-        where = []
         for slot in range(KP):
             owner = ids_ref[(pl.program_id(0) * PAIR + pair) * KP + slot] // PASS_DEV
+            for turn in range(3):
+                shift = 2 * lax.rem(turn + core, 3)
+                where[pair, slot, turn] = (owner >> shift) | ((owner << (6 - shift)) & 63)
             for channel, (kind, first, units, turn) in enumerate(CHANNELS):
-                one, two, last = lines(turn)
-                at = (coordinate(owner, last), coordinate(owner, two), coordinate(owner, one))
-                where.append(at)
                 target = values if kind else keys
                 for unit in range(units):
                     row, column = unit_place(first + unit)
                     target[pair, pl.ds(slot * PLEN + row, 16), pl.ds(column, 128)] = arrived[
                         channel
-                    ][at[0], at[1], at[2], unit]
+                    ][where[pair, slot, turn], unit]
         for head in range(4):
             columns = pl.ds(head * HEAD, HEAD)
             rows = pl.ds(head * BLK, BLK)
@@ -426,25 +431,33 @@
                 grad_ref[tokens, columns].astype(jnp.float32)
                 * gate[:, head * HEAD : (head + 1) * HEAD]
             ).astype(jnp.bfloat16)
-        expo = jnp.exp(nt(keys[pair], queries[pair]) * factor)
-        probs = expo * (1.0 / jnp.sum(expo, axis=0, keepdims=True))
-        probs_bf = probs.astype(jnp.bfloat16)
-        grad_probs = nt(values[pair], grads[pair])
-        delta = jnp.sum(probs_bf.astype(jnp.float32) * grad_probs, axis=0, keepdims=True)
-        grad_scores = (probs * (grad_probs - delta) * factor).astype(jnp.bfloat16)
-        key_grad = nn(grad_scores, queries[pair]).astype(jnp.bfloat16)
-        value_grad = nn(probs_bf, grads[pair]).astype(jnp.bfloat16)
-        query_grad = tn(grad_scores, keys[pair]).astype(jnp.bfloat16)
+    pairs = range(PAIR)
+    expo = [jnp.exp(nt(keys[pair], queries[pair]) * factor) for pair in pairs]
+    grad_probs = [nt(values[pair], grads[pair]) for pair in pairs]
+    probs = [one * (1.0 / jnp.sum(one, axis=0, keepdims=True)) for one in expo]
+    probs_bf = [one.astype(jnp.bfloat16) for one in probs]
+    delta = [
+        jnp.sum(one.astype(jnp.float32) * other, axis=0, keepdims=True)
+        for one, other in zip(probs_bf, grad_probs)
+    ]
+    grad_scores = [
+        (one * (other - third) * factor).astype(jnp.bfloat16)
+        for one, other, third in zip(probs, grad_probs, delta)
+    ]
+    for pair in pairs:
+        tokens = pl.ds(pair * BLK, BLK)
+        key_grad = nn(grad_scores[pair], queries[pair]).astype(jnp.bfloat16)
+        value_grad = nn(probs_bf[pair], grads[pair]).astype(jnp.bfloat16)
+        query_grad = tn(grad_scores[pair], keys[pair]).astype(jnp.bfloat16)
         for head in range(4):
             dq_ref[tokens, pl.ds(head * HEAD, HEAD)] = query_grad[head * BLK : (head + 1) * BLK]
         for slot in range(KP):
             for channel, (kind, first, units, turn) in enumerate(CHANNELS):
-                at = where[slot * len(CHANNELS) + channel]
                 made = value_grad if kind else key_grad
                 for unit in range(units):
                     row, column = unit_place(first + unit)
                     row = row + slot * PLEN
-                    leaving[channel][at[0], at[1], at[2], unit] = made[
+                    leaving[channel][where[pair, slot, turn], unit] = made[
                         row : row + 16, column : column + 128
                     ]
 
@@ -453,15 +466,13 @@
     bf16 = jnp.bfloat16
     length, width = q.shape
     units = [channel[2] for channel in CHANNELS]
-    whole = [
-        pl.BlockSpec((4, 4, 4, n, 16, 128), lambda step, ids: (0, 0, 0, 0, 0, 0)) for n in units
-    ]
+    whole = [pl.BlockSpec((OWNERS, n, 16, 128), lambda step, ids: (0, 0, 0, 0)) for n in units]
     rows = pl.BlockSpec((PAIR * BLK, width), lambda step, ids: (step, 0))
-    return pl.pallas_call(
+    dq, *leaving = pl.pallas_call(
         attention_kernel,
         name="cross_attention",
         out_shape=[jax.ShapeDtypeStruct((length, width), bf16)]
-        + [jax.ShapeDtypeStruct((4, 4, 4, n, 16, 128), bf16) for n in units],
+        + [jax.ShapeDtypeStruct((OWNERS, n, 16, 128), bf16) for n in units],
         grid_spec=pltpu.PrefetchScalarGridSpec(
             num_scalar_prefetch=1,
             grid=(length // (PAIR * BLK),),
@@ -470,7 +481,8 @@
             scratch_shapes=[pltpu.VMEM((PAIR, 256, 256), bf16)] * 4,
         ),
         compiler_params=pltpu.CompilerParams(vmem_limit_bytes=VMEM_LIMIT),
-    )(ids, gate, q, grad, *arrived)
+    )(ids, gate, q, grad, *[one.reshape(OWNERS, -1, 16, 128) for one in arrived])
+    return dq, [one.reshape(4, 4, 4, -1, 16, 128) for one in leaving]
 
 
 def backward_kernel(
@@ -490,7 +502,7 @@
     *rest,
 ):
     leaving = rest[:6]
-    gt_ref, gs_ref, gw_ref = rest[6:9]
+    gt_any, gs_any, out = rest[6:9]
     own, third, sums, second, fewer, first_in = (
         rest[9:15],
         rest[15:21],
@@ -525,7 +537,9 @@
         ar_first,
         ar_second,
         ar_third,
-        out,
+        gt,
+        gs,
+        flipped,
         load,
         near_send,
         near_recv,
@@ -562,46 +576,48 @@
     ]
     line_barrier(me, sibling)
 
-    def remote(stage, channel, step, dim, source, target):
+    def remote(stage, channel, step, dim, source, target, half=0):
         return pltpu.make_async_remote_copy(
             src_ref=source,
             dst_ref=target,
-            send_sem=send.at[stage, channel, step - 1],
-            recv_sem=recv.at[stage, channel, step - 1],
+            send_sem=send.at[stage, channel, step - 1, half],
+            recv_sem=recv.at[stage, channel, step - 1, half],
             device_id={"st": peer_of(me, dim, step)},
             device_id_type=MESH,
         )
 
-    def third_stage(channels):
+    def third_stage(channels, halves):
         copies = {}
         for channel in channels:
             last = lines(CHANNELS[channel][3])[2]
             at = coordinate(me, last)
-            for step in STEPS:
-                copies[channel, step] = remote(
-                    0,
-                    channel,
-                    step,
-                    last,
-                    leaving[channel].at[lax.rem(at + step, 4)],
-                    third[channel].at[step - 1],
-                )
-                copies[channel, step].start()
+            for half, rows in halves:
+                for step in STEPS:
+                    one = remote(
+                        0,
+                        channel,
+                        step,
+                        last,
+                        leaving[channel].at[lax.rem(at + step, 4), rows],
+                        third[channel].at[step - 1, rows],
+                        half,
+                    )
+                    one.start()
+                    copies[channel, half, step] = one
         return copies
 
-    def second_stage(channels, before):
-        copies = {}
+    def add_readers(channels, before, start, stop):
         for channel in channels:
             one, two, last = lines(CHANNELS[channel][3])
             here = coordinate(me, last)
-            own_loads[channel].wait()
-            for step in STEPS:
-                before[channel, step].wait()
-
-            @pl.loop(0, 16)
+            for (which, _, _), copy in before.items():
+                if which == channel:
+                    copy.wait()
+
+            @pl.loop(start * 4, stop * 4, unroll=4)
             def _(at):
                 beside, along = at // 4, lax.rem(at, 4)
-                owner = along * STRIDES[one] + beside * STRIDES[two] + here * STRIDES[last]
+                owner = along * stride(one) + beside * stride(two) + here * stride(last)
                 names = [need_ref[0, 0, owner]] + [
                     asked[last * 3 + step - 1, 0, owner] for step in STEPS
                 ]
@@ -609,30 +625,39 @@
                     third[channel][step - 1, beside, along].astype(jnp.float32) for step in STEPS
                 ]
                 for passage in range(PASS_DEV):
-                    held = jnp.zeros_like(rows[0])
-                    for name, row in zip(names, rows):
-                        held = held + row * jnp.where(name == passage, 1.0, 0.0)
+                    terms = [
+                        row * jnp.where(name == passage, 1.0, 0.0) for name, row in zip(names, rows)
+                    ]
+                    held = (terms[0] + terms[1]) + (terms[2] + terms[3])
                     sums[channel][beside, along, passage] = held.astype(jnp.bfloat16)
 
+    def second_stage(channels, halves):
+        copies = {}
+        for channel in channels:
+            _, two, _ = lines(CHANNELS[channel][3])
             at = coordinate(me, two)
-            for step in STEPS:
-                copies[channel, step] = remote(
-                    1,
-                    channel,
-                    step,
-                    two,
-                    sums[channel].at[lax.rem(at + step, 4)],
-                    second[channel].at[step - 1],
-                )
-                copies[channel, step].start()
+            for half, rows in halves:
+                for step in STEPS:
+                    one = remote(
+                        1,
+                        channel,
+                        step,
+                        two,
+                        sums[channel].at[lax.rem(at + step, 4), rows],
+                        second[channel].at[step - 1, rows],
+                        half,
+                    )
+                    one.start()
+                    copies[channel, half, step] = one
         return copies
 
     def first_stage(channels, before):
         copies = {}
         for channel in channels:
             one, two, _ = lines(CHANNELS[channel][3])
-            for step in STEPS:
-                before[channel, step].wait()
+            for (which, _, _), copy in before.items():
+                if which == channel:
+                    copy.wait()
             here = coordinate(me, two)
             held = sums[channel][here].astype(jnp.float32)
             for step in STEPS:
@@ -656,7 +681,7 @@
             _, first, units, turn = CHANNELS[channel]
             for step in STEPS:
                 before[channel, step].wait()
-            held = fewer[channel][coordinate(me, turn)].astype(jnp.float32)
+            held = fewer[channel][coordinate(me, lines(turn)[0])].astype(jnp.float32)
             for step in STEPS:
                 held = held + first_in[channel][step - 1].astype(jnp.float32)
             held = held.astype(jnp.bfloat16)
@@ -702,28 +727,39 @@
         def _(tile):
             near(tile, theirs.at[tile], passed.at[tile]).wait()
             columns = aligned(tile * 256, 256, 256)
-            gt_ref[:, columns] = (mine[tile] + passed[tile].astype(jnp.float32)).astype(
+            gt[:, columns] = (mine[tile] + passed[tile].astype(jnp.float32)).astype(
                 jnp.bfloat16
             )
 
-    keys = third_stage(KEY_CHANNELS)
-    values = third_stage(VALUE_CHANNELS)
-    for one in loads + own_loads:
+    whole = ((0, pl.ds(0, 4)),)
+    lower, upper = ((0, pl.ds(0, 2)),), ((1, pl.ds(2, 2)),)
+    keys = third_stage(KEY_CHANNELS, whole)
+    values = third_stage(VALUE_CHANNELS, lower)
+    for one in own_loads + loads:
         one.start()
     for one in loads[:8]:
         one.wait()
-    token_grads(0, 3)
-    keys = second_stage(KEY_CHANNELS, keys)
-    token_grads(3, 5)
-    values = second_stage(VALUE_CHANNELS, values)
+    token_grads(0, 2)
+    for one in own_loads:
+        one.wait()
+    waiting, keys = keys, {}
+    for channel in KEY_CHANNELS:
+        add_readers((channel,), waiting, 0, 4)
+        keys.update(second_stage((channel,), whole))
+    more = third_stage(VALUE_CHANNELS, upper)
+    loads[8].wait()
+    flipped[...] = store[...].T
+    token_grads(2, 4)
+    add_readers(VALUE_CHANNELS, values, 0, 2)
+    token_grads(4, 5)
+    keys = first_stage(KEY_CHANNELS, keys)
     token_grads(5, 6)
-    keys = first_stage(KEY_CHANNELS, keys)
-    token_grads(6, 8)
-    values = first_stage(VALUE_CHANNELS, values)
-    for one in loads[8:]:
-        one.wait()
+    waiting, values = more, {}
+    for channel in VALUE_CHANNELS:
+        add_readers((channel,), waiting, 2, 4)
+        values.update(second_stage((channel,), lower))
     passage_sums(KEY_CHANNELS, keys, key_grad)
-    term[...] = tn(store[...], key_grad[...])
+    term[...] = nn(flipped[...], key_grad[...])
     half[...] = term[...].astype(jnp.bfloat16)
 
     def ar_copy(stage, place, step, dim, source, target):
@@ -738,7 +774,8 @@
 
     started = []
     for place, (start, size) in enumerate(PARTS):
-        at = coordinate(me, place)
+        dim = lines(place)[0]
+        at = coordinate(me, dim)
         quarter = size // 4
         for step in STEPS:
             there = lax.rem(at + step, 4)
@@ -746,12 +783,66 @@
                 0,
                 place,
                 step,
-                place,
+                dim,
                 half.at[aligned(start + there * quarter, quarter)],
                 ar_first.at[step - 1, pl.ds(start // 4, quarter)],
             )
             one.start()
             started.append(one)
+    values.update(second_stage(VALUE_CHANNELS, upper))
+    token_grads(6, 8)
+    for one in loads[9:]:
+        one.wait()
+    stage = []
+    for place, (start, size) in enumerate(PARTS):
+        dim, other, _ = lines(place)
+        at, beside = coordinate(me, dim), coordinate(me, other)
+        quarter, small = size // 4, size // 16
+        base = start + at * quarter
+        for step in STEPS:
+            started[place * 3 + step - 1].wait()
+        held = term[aligned(base, quarter), :]
+        for step in STEPS:
+            held = held + ar_first[step - 1, pl.ds(start // 4, quarter), :].astype(jnp.float32)
+        total[pl.ds(start // 4, quarter), :] = held
+        half[aligned(base, quarter), :] = held.astype(jnp.bfloat16)
+        for step in STEPS:
+            there = lax.rem(beside + step, 4)
+            one = ar_copy(
+                1,
+                place,
+                step,
+                other,
+                half.at[aligned(base + there * small, small)],
+                ar_second.at[step - 1, pl.ds(start // 16, small)],
+            )
+            one.start()
+            stage.append(one)
+    values = first_stage(VALUE_CHANNELS, values)
+    token_ends(0, 4)
+    started, stage = stage, []
+    for place, (start, size) in enumerate(PARTS):
+        dim, other, last = lines(place)
+        at, beside = coordinate(me, dim), coordinate(me, other)
+        quarter, small = size // 4, size // 16
+        base = start + at * quarter + beside * small
+        for step in STEPS:
+            started[place * 3 + step - 1].wait()
+        held = total[aligned(start // 4 + beside * small, small), :]
+        for step in STEPS:
+            held = held + ar_second[step - 1, pl.ds(start // 16, small), :].astype(jnp.float32)
+        half[aligned(base, small), :] = held.astype(jnp.bfloat16)
+        for step in STEPS:
+            one = ar_copy(
+                2,
+                place,
+                step,
+                last,
+                half.at[aligned(base, small)],
+                ar_third.at[step - 1, pl.ds(start // 16, small)],
+            )
+            one.start()
+            stage.append(one)
     passage_sums(VALUE_CHANNELS, values, value_grad)
     store_rows = 2 * PLEN
     made = nt(
@@ -777,60 +868,13 @@
     store_mine[...] = made[store_rows:]
     store_near = near(8, store_theirs, store_passed)
     store_near.start()
-    stage = []
-    for place, (start, size) in enumerate(PARTS):
-        other = (place + 1) % 3
-        at, beside = coordinate(me, place), coordinate(me, other)
-        quarter, small = size // 4, size // 16
-        base = start + at * quarter
-        for step in STEPS:
-            started[place * 3 + step - 1].wait()
-        held = term[aligned(base, quarter), :]
-        for step in STEPS:
-            held = held + ar_first[step - 1, pl.ds(start // 4, quarter), :].astype(jnp.float32)
-        total[pl.ds(start // 4, quarter), :] = held
-        half[aligned(base, quarter), :] = held.astype(jnp.bfloat16)
-        for step in STEPS:
-            there = lax.rem(beside + step, 4)
-            one = ar_copy(
-                1,
-                place,
-                step,
-                other,
-                half.at[aligned(base + there * small, small)],
-                ar_second.at[step - 1, pl.ds(start // 16, small)],
-            )
-            one.start()
-            stage.append(one)
-    token_ends(0, 4)
+    token_ends(4, 8)
+    ends = [pltpu.make_async_copy(gt, gt_any, load.at[17])]
+    ends[0].start()
     started, stage = stage, []
     for place, (start, size) in enumerate(PARTS):
-        _, other, last = lines(place)
-        at, beside = coordinate(me, place), coordinate(me, other)
-        quarter, small = size // 4, size // 16
-        base = start + at * quarter + beside * small
-        for step in STEPS:
-            started[place * 3 + step - 1].wait()
-        held = total[aligned(start // 4 + beside * small, small), :]
-        for step in STEPS:
-            held = held + ar_second[step - 1, pl.ds(start // 16, small), :].astype(jnp.float32)
-        half[aligned(base, small), :] = held.astype(jnp.bfloat16)
-        for step in STEPS:
-            one = ar_copy(
-                2,
-                place,
-                step,
-                last,
-                half.at[aligned(base, small)],
-                ar_third.at[step - 1, pl.ds(start // 16, small)],
-            )
-            one.start()
-            stage.append(one)
-    token_ends(4, 8)
-    started, stage = stage, []
-    for place, (start, size) in enumerate(PARTS):
-        other = (place + 1) % 3
-        at, beside = coordinate(me, place), coordinate(me, other)
+        dim, other, _ = lines(place)
+        at, beside = coordinate(me, dim), coordinate(me, other)
         quarter, small = size // 4, size // 16
         base = start + at * quarter + beside * small
         for step in STEPS:
@@ -849,22 +893,24 @@
             one.start()
             stage.append(one)
     store_near.wait()
-    gs_ref[...] = (store_mine[...] + store_passed[...].astype(jnp.float32)).astype(jnp.bfloat16)
+    gs[...] = (store_mine[...] + store_passed[...].astype(jnp.float32)).astype(jnp.bfloat16)
+    ends.append(pltpu.make_async_copy(gs, gs_any, load.at[18]))
+    ends[1].start()
     started, stage = stage, []
     for place, (start, size) in enumerate(PARTS):
-        at = coordinate(me, place)
+        dim = lines(place)[0]
+        at = coordinate(me, dim)
         quarter = size // 4
         base = start + at * quarter
         for step in STEPS:
             started[place * 3 + step - 1].wait()
         for step in STEPS:
             here = out.at[aligned(base, quarter)]
-            one = ar_copy(4, place, step, place, here, here)
+            one = ar_copy(4, place, step, dim, here, here)
             one.start()
             stage.append(one)
-    for one in stage:
+    for one in stage + ends:
         one.wait()
-    gw_ref[...] = out[...].astype(jnp.float32)
 
 
 def backward(
@@ -901,12 +947,14 @@
             pltpu.VMEM((3, width // 4, kv_width), bf16),
             pltpu.VMEM((3, width // 16, kv_width), bf16),
             pltpu.VMEM((3, width // 16, kv_width), bf16),
-            pltpu.VMEM((width, kv_width), bf16),
-            pltpu.SemaphoreType.DMA((17,)),
+            pltpu.VMEM((length // 2, width), bf16),
+            pltpu.VMEM((2 * PLEN, width), bf16),
+            pltpu.VMEM((width, PASS_DEV * PLEN), bf16),
+            pltpu.SemaphoreType.DMA((19,)),
             pltpu.SemaphoreType.DMA((9,)),
             pltpu.SemaphoreType.DMA((9,)),
-            pltpu.SemaphoreType.DMA((3, 6, 3)),
-            pltpu.SemaphoreType.DMA((3, 6, 3)),
+            pltpu.SemaphoreType.DMA((3, 6, 3, 2)),
+            pltpu.SemaphoreType.DMA((3, 6, 3, 2)),
             pltpu.SemaphoreType.DMA((5, 3, 3)),
             pltpu.SemaphoreType.DMA((5, 3, 3)),
         ]
@@ -917,15 +965,40 @@
         out_shape=[
             jax.ShapeDtypeStruct((length // 2, width), bf16),
             jax.ShapeDtypeStruct((2 * PLEN, width), bf16),
-            jax.ShapeDtypeStruct((width, kv_width), f32),
+            jax.ShapeDtypeStruct((width, kv_width), bf16),
         ],
         in_specs=[smem_spec(), smem_spec()] + [any_spec()] * 17,
-        out_specs=[vmem_spec()] * 3,
+        out_specs=[any_spec(), any_spec(), vmem_spec()],
         scratch_shapes=scratch,
         compiler_params=pltpu.CompilerParams(
             collective_id=1, has_side_effects=True, vmem_limit_bytes=VMEM_LIMIT
         ),
     )(need, asked, store, w_key, w_value, dq, grq, grk, grv, w_q, w_rq, w_rk, w_rv, *leaving)
+
+
+def finish_kernel(gt_in, gs_in, gw_in, gt_ref, gs_ref, gw_ref):
+    gt_ref[...] = gt_in[...]
+    gs_ref[...] = gs_in[...]
+    gw_ref[...] = gw_in[...].astype(jnp.float32)
+
+
+def finish(*arrays):
+    steps = 4
+    specs = [
+        pl.BlockSpec((array.shape[0] // steps, array.shape[1]), lambda step: (step, 0))
+        for array in arrays
+    ]
+    return pl.pallas_call(
+        finish_kernel,
+        name="finish",
+        out_shape=[
+            jax.ShapeDtypeStruct(array.shape, dtype)
+            for array, dtype in zip(arrays, (jnp.bfloat16, jnp.bfloat16, jnp.float32))
+        ],
+        grid=(steps,),
+        in_specs=specs,
+        out_specs=specs,
+    )(*arrays)
 
 
 def per_device(
@@ -966,8 +1039,8 @@
         out_grad,
     )
     arrived, (asked, q, grq, grk, grv) = made[:6], made[6:]
-    dq, *leaving = attention(ids, gate_logit.reshape(1, -1), q, out_grad, arrived)
-    grad_tokens, grad_store, grad_key_weight = backward(
+    dq, leaving = attention(ids, gate_logit.reshape(1, -1), q, out_grad, arrived)
+    made = backward(
         need,
         asked,
         store_rows,
@@ -983,6 +1056,7 @@
         w_ret_value,
         leaving,
     )
+    grad_tokens, grad_store, grad_key_weight = finish(*made)
     return (grad_tokens, grad_store.reshape(-1, PLEN, width), grad_key_weight)
 
 

time: 141 us -> 135 us (0.957)
  local copies, waits for them, and re-layouts: 6.28 us -> 0.85 us
    unnamed x10 -> x3, local copies, waits for them, and re-layouts: 6.19 us -> 0.76 us
    pallas_call x0 -> x1, Pallas kernels: none -> 4.69 us  [finish(): pl.pallas_call(finish_kernel, name='finish', out_shape=[jax.ShapeDtypeStr...]
    pallas_call x1, Pallas kernels: 13.5 us -> 10.5 us  [attention(): pl.pallas_call(attention_kernel, name='cross_attention', out_shape=[jax.S...]
    pallas_call x1, Pallas kernels: 51.7 us -> 49.3 us  [forward(): pl.pallas_call(forward_kernel, name='fetch_and_retain', out_shape=out_sha...]
where the time goes in v2:
time: 135 us; the launch traced here: 134 us
  Pallas kernels  132 us (98%)
    pallas_call x1, Pallas kernels, backward(): pl.pallas_call(backward_kernel, name='return_and_reduce', out_shape=[jax....  67.6 us
    pallas_call x1, Pallas kernels, forward(): pl.pallas_call(forward_kernel, name='fetch_and_retain', out_shape=out_sha...  49.3 us
    pallas_call x1, Pallas kernels, attention(): pl.pallas_call(attention_kernel, name='cross_attention', out_shape=[jax.S...  10.5 us
    pallas_call x1, Pallas kernels, finish(): pl.pallas_call(finish_kernel, name='finish', out_shape=[jax.ShapeDtypeStr...  4.69 us

profile of v2, /device:TPU:0, one launch (start us, length us, event | category | flops | bytes accessed | tf_op | source)
XLA Modules:
  0.0 134.2 jit_solution(620153871564598776)
XLA Ops:
  0.6 0.8 copy.18
  1.4 0.1 reshape.109.ids_ref
  1.5 0.0 copy-start
  1.5 0.6 select_reduce_fusion
  2.1 49.3 %fetch_and_retain.1 = (bf16[4,4,4,3,16,128]{5,4,3,2,1,0:T(8,128)(2,1)}, bf16[4,4,4,3,16,128]{5,4,3,2,1,0:T(8,128)(2,1)}, bf16[4,4,4,2,16,128]{5,4,3,2,1,0:T(8,12...) custom-call(s32[1,1,128]{2,1,0:T(1,128)} %bitcast.33, ...), custom_call_target="tpu_custom_call" | custom-call | tf_op jit(solution)/shard_map/fetch_and_retain/pallas_call | solution.py:389
  51.5 0.0 copy-done
  51.5 10.5 %cross_attention.1 = (bf16[1024,1024]{1,0:T(8,128)(2,1)}, bf16[64,3,16,128]{3,2,1,0:T(8,128)(2,1)}, bf16[64,3,16,128]{3,2,1,0:T(8,128)(2,1)}, bf16[64,2,16,128]{...) custom-call(s32[64]{0:T(128)} %copy-done, ...), custom_call_target="tpu_custom_call" | custom-call | tf_op jit(solution)/shard_map/cross_attention/pallas_call | solution.py:471
  61.9 67.6 %return_and_reduce.1 = (bf16[512,2048]{1,0:T(8,128)(2,1)}, bf16[128,2048]{1,0:T(8,128)(2,1)}, bf16[2048,256]{1,0:T(8,128)(2,1)}) custom-call(s32[1,1,128]{2,1,0:T(1,128)} %bitcast.34, s32[9,1,128]{2,1,0:T(1,128)} %get-tuple-element.27.asked, bf16[256,2048]{1,0:T(8,128)(2,1)} %bitcast.18, bf16[2048,256]{1,0:T(8,128)(2,1)} %w_key_any.3, ...), custom_call_target="tpu_custom_call" | custom-call | tf_op jit(solution)/shard_map/return_and_reduce/pallas_call | solution.py:962
  129.5 4.7 %finish.1 = (bf16[512,2048]{1,0:T(8,128)(2,1)}, bf16[128,2048]{1,0:T(8,128)(2,1)}, f32[2048,256]{1,0:T(8,128)}) custom-call(bf16[512,2048]{1,0:T(8,128)(2,1)} %get-tuple-element.45.gt_in, bf16[128,2048]{1,0:T(8,128)(2,1)} %get-tuple-element.46.gs_in, bf16[2048,256]{1,0:T(8,128)(2,1)} %get-tuple-element.47.gw_in), custom_call_target="tpu_custom_call" | custom-call | tf_op jit(solution)/shard_map/finish/pallas_call | solution.py:991
  (1 shorter events, 0.0 us)
Async XLA Ops:
  1.5 50.0 %copy-start = (s32[64]{0:T(128)}, s32[64]{0:T(128)S(1)}, u32[]{:S(2)}) copy-start(s32[64]{0:T(128)S(1)} %reshape.109.ids_ref) | copy-start | bytes 772
